TPU v7x, 32 devices: a whole 2x2x4 slice. The times are simulated.
32 devices in a mesh: sp: 16 (over z, y, x), tp: 2 (over core).
Axes of the slice: x: 2, y: 2, z: 4, core: 2. Of those that a mesh axis runs over, the one named last changes fastest.
Arguments:
- value_in: bfloat16 [4096, 2048], P('sp', 'tp'), may hold values from -25 to 25, as said below
- gate_in: bfloat16 [4096, 2048], P('sp', 'tp'), may hold values from -6 to 6
- taps: float32 [31, 2048], P(None, 'tp'), may hold values from -1 to 1
- gain: float32 [2048], P('tp'), may hold values from 0.1 to 1.9
- shift: float32 [2048], P('tp'), may hold values from -3 to 3
- w_out: bfloat16 [2048, 2048], P('tp'), may hold values from -0.125 to 0.125
- grad_out: bfloat16 [4096, 2048], P('sp'), may hold values from -6 to 6
Outputs:
- d_value: bfloat16 [4096, 2048], P('sp', 'tp')
- d_gate: bfloat16 [4096, 2048], P('sp', 'tp')
- d_taps: float32 [31, 2048], P(None, 'tp')
- d_gain: float32 [2048], P('tp')
- d_shift: float32 [2048], P('tp')
Inputs may be any that keep to these rules, and one draw needn't show every extreme that they name: `value_in`: channel blocks of different magnitude.
All inputs are finite; a program needn't handle non-finite values.
Results may differ from a plain program's by a relative error of at most 0.007.
Values may be sent and summed in bfloat16 or wider, within the bound.
A program may use at most 64 MiB of HBM per device.

v0:
```python
import functools
import math

import jax
import jax.numpy as jnp
import numpy as np
from jax import lax
from jax.experimental import pallas as pl
from jax.experimental.pallas import tpu as pltpu
from jax.sharding import PartitionSpec as P

EPS = 1e-05
ALIGN = 16
LANES = 128
CHUNK = 256
VMEM_GRANT = 62 * 1024 * 1024
F32 = jnp.float32
BF16 = jnp.bfloat16


class Plan:
    def __init__(self, rows, kernel, total):
        self.half = kernel // 2
        self.kernel = kernel
        self.rows = rows
        self.edge = -(-(self.half + 1) // ALIGN) * ALIGN
        edge = self.edge
        self.size = rows // 2 + 4 * edge
        size = self.size
        self.freqs = size // 2
        self.wide = rows + 4 * edge
        self.mid = rows + 2 * edge
        self.fwd_out = self.mid // 2
        self.fwd_step = self.wide - size
        self.bwd_out = rows // 2
        self.bwd_step = self.mid - size
        omega = 2.0 * np.pi * (np.arange(self.freqs) + 0.5) / size

        def spectrum(times):
            angle = omega[:, None] * times[None, :]
            return np.concatenate([np.cos(angle), np.sin(angle)], 0)

        def inverse(times):
            angle = times[:, None] * omega[None, :]
            return np.concatenate([np.cos(angle), -np.sin(angle)], 1)

        forward = spectrum(np.arange(size))
        conv = []
        grad = []
        own = []
        for b in range(2):
            start = b * self.fwd_out + edge - self.half - b * self.fwd_step
            conv.append(inverse(np.arange(self.fwd_out) + start))
            start = b * self.bwd_out + edge + self.half - b * self.bwd_step
            grad.append(inverse(np.arange(self.bwd_out) + start))
            start = b * self.bwd_out + edge - b * self.bwd_step
            own.append(spectrum(np.arange(self.bwd_out) + start))
        self.tap_rows = -(-kernel // ALIGN) * ALIGN
        lags = inverse(np.arange(self.tap_rows) - self.half)
        lags[kernel:] = 0.0
        self.mats = np.concatenate([forward] + conv + grad + [lags], 0)
        self.at_conv = size
        self.at_grad = self.at_conv + self.mid
        self.at_lags = self.at_grad + rows
        self.own = np.concatenate(own, 0)
        self.taps = spectrum(np.arange(kernel)) * (2.0 / size)
        self.lag_scale = 2.0 / size / math.sqrt(total)


def dot(a, b):
    return jnp.dot(a, b, preferred_element_type=F32)


def sigmoid(x):
    return 0.5 * jnp.tanh(0.5 * x) + 0.5


def body(
    plan, n, tiles, per, total,
    value_h, gate_h, taps_h, gain_h, shift_h, w_h, go_h, mats_h, own_h, ft_h,
    dv_h, dg_h, dt_o, dgs_o,
    value, gate, taps, gain, shift, w, go, mats, own, ft,
    sig_s, gw, conv, gm, gcw, ts, hs, gs_spec, acc1, acc2,
    st1, st1_in, st2, st2_in, inv_s, colg, cols,
    gs, rs_src, rs_in, ag, dv, dg,
    load_sem, w_sem, out_sem, halo_send, halo_recv, tp_send, tp_recv,
    all_send, all_recv,
):
    sp = lax.axis_index("sp")
    tp = lax.axis_index("tp")
    rows, edge, half2 = plan.rows, plan.edge, 2 * plan.edge
    channels = value.shape[1]
    width = channels * 2
    chunks = channels // CHUNK
    size, freqs, mid = plan.size, plan.freqs, plan.mid
    nxt = lax.rem(sp + 1, n)
    prv = lax.rem(sp + n - 1, n)

    def peer(d):
        return lax.rem(sp + d, n)

    barrier = pltpu.get_barrier_semaphore()

    def greet(d, carry):
        pl.semaphore_signal(
            barrier, 1, device_id=(peer(d), tp), device_id_type=pl.DeviceIdType.MESH
        )
        return carry

    pl.semaphore_signal(
        barrier, 1, device_id=(sp, 1 - tp), device_id_type=pl.DeviceIdType.MESH
    )
    lax.fori_loop(1, n, greet, 0)

    own_go = go.at[pl.ds(edge, rows)]
    pairs = [
        (value_h, value), (gate_h, gate), (taps_h, taps), (ft_h, ft), (own_h, own),
        (mats_h, mats), (go_h, own_go), (gain_h, gain), (shift_h, shift),
    ]
    loads = [
        pltpu.make_async_copy(a, b, load_sem.at[i]) for i, (a, b) in enumerate(pairs)
    ]
    for load in loads:
        load.start()

    def w_copy(c):
        part = pl.ds(pl.multiple_of(c * CHUNK, CHUNK), CHUNK)
        return pltpu.make_async_copy(w_h.at[part], w.at[part], w_sem.at[c])

    for c in range(chunks):
        w_copy(c).start()

    def cut(c):
        return pl.ds(pl.multiple_of(c * CHUNK, CHUNK), CHUNK)

    loads[0].wait()
    loads[1].wait()

    def gate_step(i, carry):
        part = pl.ds(pl.multiple_of(i * ALIGN, ALIGN), ALIGN)
        place = pl.ds(pl.multiple_of(i * ALIGN + half2, ALIGN), ALIGN)
        sig = sigmoid(gate[part].astype(F32))
        sig_s[part] = sig
        gw[place] = (value[part].astype(F32) * sig).astype(BF16)
        return carry

    lax.fori_loop(0, rows // ALIGN, gate_step, 0, unroll=4)
    for load in loads[2:7]:
        load.wait()

    def tap_step(c, carry):
        ts[:, cut(c)] = jnp.dot(
            ft[...], taps[:, cut(c)], precision=lax.Precision.HIGHEST,
            preferred_element_type=F32,
        )
        return carry

    lax.fori_loop(0, chunks, tap_step, 0, unroll=2)

    pl.semaphore_wait(barrier, n)

    def remote(src, dst, send, recv, device):
        return pltpu.make_async_remote_copy(
            src_ref=src, dst_ref=dst, send_sem=send, recv_sem=recv,
            device_id=device, device_id_type=pl.DeviceIdType.MESH,
        )

    halos = [
        remote(gw.at[pl.ds(rows, half2)], gw.at[pl.ds(0, half2)],
               halo_send.at[0], halo_recv.at[0], (nxt, tp)),
        remote(gw.at[pl.ds(half2, half2)], gw.at[pl.ds(rows + half2, half2)],
               halo_send.at[1], halo_recv.at[1], (prv, tp)),
        remote(go.at[pl.ds(rows, edge)], go.at[pl.ds(0, edge)],
               halo_send.at[2], halo_recv.at[2], (nxt, tp)),
        remote(go.at[pl.ds(edge, edge)], go.at[pl.ds(rows + edge, edge)],
               halo_send.at[3], halo_recv.at[3], (prv, tp)),
    ]
    for halo in halos:
        halo.start()

    def mix(a, b):
        return lax.dot_general(a, b, (((1,), (1,)), ((), ())), preferred_element_type=F32)

    def own_step(c, carry):
        for b in range(2):
            hs[pl.ds(b * size, size), cut(c)] = dot(
                own[pl.ds(b * size, size)],
                gw[pl.ds(half2 + b * plan.bwd_out, plan.bwd_out), cut(c)],
            )
        return carry

    lax.fori_loop(0, chunks, own_step, 0, unroll=2)

    def mix_step(c, carry):
        w_copy(c).wait()
        gm[pl.ds(edge, rows), cut(c)] = mix(go[pl.ds(edge, rows)], w[cut(c)])
        return carry

    lax.fori_loop(0, chunks, mix_step, 0)

    halos[0].wait_recv()
    halos[1].wait_recv()

    @pl.when(sp == 0)
    def _():
        gw[pl.ds(0, half2)] = jnp.zeros((half2, channels), BF16)

    @pl.when(sp == n - 1)
    def _():
        gw[pl.ds(rows + half2, half2)] = jnp.zeros((half2, channels), BF16)

    acc1[...] = jnp.zeros_like(acc1)
    acc2[...] = jnp.zeros_like(acc2)

    def fold(x):
        out = x[:, :LANES]
        for k in range(1, x.shape[1] // LANES):
            out = out + x[:, k * LANES : (k + 1) * LANES]
        return out

    def conv_step(c, carry):
        ta = ts[pl.ds(0, freqs), cut(c)]
        tb = ts[pl.ds(freqs, freqs), cut(c)]
        for b in range(2):
            spec = dot(mats[pl.ds(0, size)], gw[pl.ds(b * plan.fwd_step, size), cut(c)])
            re, im = spec[:freqs], spec[freqs:]
            prod = jnp.concatenate([re * ta + im * tb, re * tb - im * ta], 0).astype(BF16)
            out = dot(mats[pl.ds(plan.at_conv + b * plan.fwd_out, plan.fwd_out)], prod)
            place = pl.ds(b * plan.fwd_out, plan.fwd_out)
            conv[place, cut(c)] = out
            acc1[place] += fold(out)
            acc2[place] += fold(out * out)
        return carry

    lax.fori_loop(0, chunks, conv_step, 0, unroll=2)

    first_lanes = lax.broadcasted_iota(jnp.int32, (mid, LANES), 1) < LANES // 2
    st1[...] = jnp.where(
        first_lanes,
        jnp.sum(acc1[...], 1, keepdims=True),
        jnp.sum(acc2[...], 1, keepdims=True),
    )
    swap1 = remote(st1, st1_in, tp_send.at[0], tp_recv.at[0], (sp, 1 - tp))
    swap1.start()

    halos[2].wait_recv()
    halos[3].wait_recv()

    def edge_step(c, carry):
        both = jnp.concatenate([go[pl.ds(0, edge)], go[pl.ds(rows + edge, edge)]], 0)
        out = mix(both, w[cut(c)])
        gm[pl.ds(0, edge), cut(c)] = out[:edge]
        gm[pl.ds(rows + edge, edge), cut(c)] = out[edge:]
        return carry

    lax.fori_loop(0, chunks, edge_step, 0)
    loads[7].wait()
    loads[8].wait()
    colg[...] = jnp.zeros_like(colg)
    cols[...] = jnp.zeros_like(cols)
    swap1.wait_recv()
    lanes = lax.broadcasted_iota(jnp.int32, (ALIGN, LANES), 1) < LANES // 2

    def norm_step(i, carry):
        part = pl.ds(pl.multiple_of(i * ALIGN, ALIGN), ALIGN)
        tot = (st1[part] + st1_in[part]) * (1.0 / width)
        mean = tot[:, :1]
        var = tot[:, LANES // 2 : LANES // 2 + 1] - mean * mean
        inv = lax.rsqrt(var + EPS)
        normed = (conv[part] - mean) * inv
        pre = normed * gain[...] + shift[...]
        sig = sigmoid(pre)
        gp = gm[part] * sig * (1.0 + pre * (1.0 - sig))
        gn = gp * gain[...]
        conv[part] = normed
        gm[part] = gn
        gx = gn * normed
        st2[part] = jnp.where(
            lanes,
            jnp.sum(fold(gn), 1, keepdims=True),
            jnp.sum(fold(gx), 1, keepdims=True),
        )
        inv_s[part] = jnp.broadcast_to(inv, (ALIGN, LANES))

        inside = (i >= edge // ALIGN) & (i < (rows + edge) // ALIGN)
        gpn = gp * normed
        colg[...] += jnp.where(inside, gpn[:8] + gpn[8:], 0.0)
        cols[...] += jnp.where(inside, gp[:8] + gp[8:], 0.0)
        return carry

    lax.fori_loop(0, mid // ALIGN, norm_step, 0, unroll=3)
    swap2 = remote(st2, st2_in, tp_send.at[1], tp_recv.at[1], (sp, 1 - tp))
    swap2.start()

    rg = jnp.sum(colg[...], 0, keepdims=True)
    rsh = jnp.sum(cols[...], 0, keepdims=True)
    groups = channels // LANES
    for k in range(groups):
        gs[sp, pl.ds(k, 1), :] = rg[:, k * LANES : (k + 1) * LANES]
        gs[sp, pl.ds(groups + k, 1), :] = rsh[:, k * LANES : (k + 1) * LANES]

    def send_gs(d, carry):
        remote(gs.at[sp], gs.at[sp], all_send.at[0], all_recv.at[0], (peer(d), tp)).start()
        return carry

    lax.fori_loop(1, n, send_gs, 0)
    swap2.wait_recv()

    def gc_step(i, carry):
        part = pl.ds(pl.multiple_of(i * ALIGN, ALIGN), ALIGN)
        tot = (st2[part] + st2_in[part]) * (1.0 / width)
        m1 = tot[:, :1]
        m2 = tot[:, LANES // 2 : LANES // 2 + 1]
        inv = inv_s[part][:, :1]
        gcw[part] = (inv * (gm[part] - m1 - conv[part] * m2)).astype(BF16)
        return carry

    lax.fori_loop(0, mid // ALIGN, gc_step, 0, unroll=6)

    @pl.when(sp == 0)
    def _():
        gcw[pl.ds(0, edge)] = jnp.zeros((edge, channels), BF16)

    @pl.when(sp == n - 1)
    def _():
        gcw[pl.ds(rows + edge, edge)] = jnp.zeros((edge, channels), BF16)

    if n * per > tiles:
        rs_src[pl.ds(tiles, n * per - tiles)] = jnp.zeros(
            (n * per - tiles, ALIGN, LANES), BF16
        )

    def spec_step(c, carry):
        dr = jnp.zeros((freqs, CHUNK), F32)
        di = jnp.zeros((freqs, CHUNK), F32)
        for b in range(2):
            spec = dot(mats[pl.ds(0, size)], gcw[pl.ds(b * plan.bwd_step, size), cut(c)])
            gs_spec[pl.ds(b * size, size), cut(c)] = spec
            re, im = spec[:freqs], spec[freqs:]
            hr = hs[pl.ds(b * size, freqs), cut(c)]
            hi = hs[pl.ds(b * size + freqs, freqs), cut(c)]
            dr = dr + hr * re + hi * im
            di = di + hr * im - hi * re
        prod = jnp.concatenate([dr, di], 0).astype(BF16)
        out = dot(mats[pl.ds(plan.at_lags, plan.tap_rows)], prod) * plan.lag_scale
        out = out.astype(BF16)
        for r in range(plan.tap_rows // ALIGN):
            for k in range(CHUNK // LANES):
                rs_src[r * groups + c * (CHUNK // LANES) + k] = out[
                    r * ALIGN : (r + 1) * ALIGN, k * LANES : (k + 1) * LANES
                ]
        return carry

    lax.fori_loop(0, chunks, spec_step, 0, unroll=2)

    def send_rs(d, carry):
        to = peer(d)
        remote(rs_src.at[pl.ds(to * per, per)], rs_in.at[sp],
               all_send.at[1], all_recv.at[1], (to, tp)).start()
        return carry

    lax.fori_loop(1, n, send_rs, 0)
    rs_in[sp] = rs_src[pl.ds(sp * per, per)]

    def out_step(c, carry):
        ta = ts[pl.ds(0, freqs), cut(c)]
        tb = ts[pl.ds(freqs, freqs), cut(c)]
        for b in range(2):
            re = gs_spec[pl.ds(b * size, freqs), cut(c)]
            im = gs_spec[pl.ds(b * size + freqs, freqs), cut(c)]
            prod = jnp.concatenate([re * ta - im * tb, -(re * tb + im * ta)], 0).astype(BF16)
            out = dot(mats[pl.ds(plan.at_grad + b * plan.bwd_out, plan.bwd_out)], prod)
            place = pl.ds(b * plan.bwd_out, plan.bwd_out)
            sig = sig_s[place, cut(c)]
            left = out * sig
            dv[place, cut(c)] = left.astype(BF16)
            dg[place, cut(c)] = (
                left * value[place, cut(c)].astype(F32) * (1.0 - sig)
            ).astype(BF16)
        return carry

    lax.fori_loop(0, chunks, out_step, 0, unroll=2)
    outs = [
        pltpu.make_async_copy(dv, dv_h, out_sem.at[0]),
        pltpu.make_async_copy(dg, dg_h, out_sem.at[1]),
    ]
    for out in outs:
        out.start()

    def settle(ref, k):
        part = ref.at[pl.ds(0, n - 1)]
        pltpu.make_async_copy(part, part, all_recv.at[k]).wait()

    def settle_sent(ref, k):
        part = ref.at[pl.ds(0, n - 1)]
        pltpu.make_async_copy(part, part, all_send.at[k]).wait()

    settle(rs_in, 1)
    zero = jnp.zeros((per, ALIGN, LANES), F32)
    summed = lax.fori_loop(0, n, lambda i, t: t + rs_in[i].astype(F32), zero)
    ag[sp] = summed.astype(BF16)

    def send_ag(d, carry):
        remote(ag.at[sp], ag.at[sp], all_send.at[2], all_recv.at[2], (peer(d), tp)).start()
        return carry

    lax.fori_loop(1, n, send_ag, 0)

    settle(gs, 0)
    small = lax.fori_loop(
        0, n, lambda i, t: t + gs[i], jnp.zeros(gs.shape[1:], F32)
    )
    dgs_o[...] = small * (1.0 / math.sqrt(total))

    for halo in halos:
        halo.wait_send()
    swap1.wait_send()
    swap2.wait_send()
    settle_sent(gs, 0)
    settle_sent(rs_in, 1)
    settle(ag, 2)
    for t in range(tiles):
        r, k = t // groups, t % groups
        count = min(ALIGN, plan.kernel - r * ALIGN)
        dt_o[pl.ds(r * ALIGN, count), pl.ds(k * LANES, LANES)] = ag[t // per, t % per].astype(F32)[
            :count
        ]
    settle_sent(ag, 2)
    for out in outs:
        out.wait()


def store(*refs):
    sources, targets, holds = refs[:4], refs[4:9], refs[9:13]
    in_sem, out_sem = refs[13:]
    groups = holds[3].shape[0] // 2
    views = list(holds[:3]) + [
        holds[3].at[pl.ds(0, groups)], holds[3].at[pl.ds(groups, groups)]
    ]
    loads = [
        pltpu.make_async_copy(a, b, in_sem.at[i]) for i, (a, b) in enumerate(zip(sources, holds))
    ]
    copies = [
        pltpu.make_async_copy(a, b, out_sem.at[i]) for i, (a, b) in enumerate(zip(views, targets))
    ]
    for load in loads:
        load.start()
    for i, copy in enumerate(copies):
        if i < len(loads):
            loads[i].wait()
        copy.start()
    for copy in copies:
        copy.wait()


def shards(n, value_in, gate_in, taps, gain, shift, w_out, grad_out):
    rows, channels = value_in.shape
    kernel = taps.shape[0]
    total = rows * n
    plan = Plan(rows, kernel, total)
    groups = channels // LANES
    tiles = plan.tap_rows // ALIGN * groups
    per = -(-tiles // n)
    model = grad_out.shape[1]
    mats = jnp.asarray(plan.mats, BF16)
    own = jnp.asarray(plan.own, BF16)
    ft = jnp.asarray(plan.taps, F32)
    hbm = pl.BlockSpec(memory_space=pltpu.HBM)
    vmem = pl.BlockSpec(memory_space=pltpu.VMEM)
    size, mid = plan.size, plan.mid
    chunks = channels // CHUNK
    dma = pltpu.SemaphoreType.DMA
    results = pl.pallas_call(
        functools.partial(body, plan, n, tiles, per, total),
        out_shape=(
            jax.ShapeDtypeStruct((rows, channels), BF16),
            jax.ShapeDtypeStruct((rows, channels), BF16),
            jax.ShapeDtypeStruct((kernel, channels), F32),
            jax.ShapeDtypeStruct((2 * groups, LANES), F32),
        ),
        in_specs=[hbm] * 10,
        out_specs=(hbm, hbm, vmem, vmem),
        scratch_shapes=[
            pltpu.VMEM((rows, channels), BF16),
            pltpu.VMEM((rows, channels), BF16),
            pltpu.VMEM((kernel, channels), F32),
            pltpu.VMEM((1, channels), F32),
            pltpu.VMEM((1, channels), F32),
            pltpu.VMEM((channels, model), BF16),
            pltpu.VMEM((mid, model), BF16),
            pltpu.VMEM(plan.mats.shape, BF16),
            pltpu.VMEM(plan.own.shape, BF16),
            pltpu.VMEM(plan.taps.shape, F32),
            pltpu.VMEM((rows, channels), F32),
            pltpu.VMEM((plan.wide, channels), BF16),
            pltpu.VMEM((mid, channels), F32),
            pltpu.VMEM((mid, channels), F32),
            pltpu.VMEM((mid, channels), BF16),
            pltpu.VMEM((size, channels), F32),
            pltpu.VMEM((2 * size, channels), F32),
            pltpu.VMEM((2 * size, channels), F32),
            pltpu.VMEM((mid, LANES), F32),
            pltpu.VMEM((mid, LANES), F32),
            pltpu.VMEM((mid, LANES), F32),
            pltpu.VMEM((mid, LANES), F32),
            pltpu.VMEM((mid, LANES), F32),
            pltpu.VMEM((mid, LANES), F32),
            pltpu.VMEM((mid, LANES), F32),
            pltpu.VMEM((8, channels), F32),
            pltpu.VMEM((8, channels), F32),
            pltpu.VMEM((n, 2 * groups, LANES), F32),
            pltpu.VMEM((n * per, ALIGN, LANES), BF16),
            pltpu.VMEM((n, per, ALIGN, LANES), BF16),
            pltpu.VMEM((n, per, ALIGN, LANES), BF16),
            pltpu.VMEM((rows, channels), BF16),
            pltpu.VMEM((rows, channels), BF16),
            dma((9,)), dma((chunks,)), dma((2,)), dma((4,)), dma((4,)),
            dma((2,)), dma((2,)), dma((3,)), dma((3,)),
        ],
        compiler_params=pltpu.CompilerParams(
            collective_id=0, has_side_effects=True, vmem_limit_bytes=VMEM_GRANT
        ),
    )(
        value_in, gate_in, taps, gain.reshape(1, -1), shift.reshape(1, -1), w_out,
        grad_out, mats, own, ft,
    )
    d_value, d_gate, d_taps, d_gain, d_shift = pl.pallas_call(
        store,
        out_shape=(
            jax.ShapeDtypeStruct((rows, channels), BF16),
            jax.ShapeDtypeStruct((rows, channels), BF16),
            jax.ShapeDtypeStruct((kernel, channels), F32),
            jax.ShapeDtypeStruct((groups, LANES), F32),
            jax.ShapeDtypeStruct((groups, LANES), F32),
        ),
        in_specs=[hbm] * 4,
        out_specs=(hbm,) * 5,
        scratch_shapes=[
            pltpu.VMEM((rows, channels), BF16),
            pltpu.VMEM((rows, channels), BF16),
            pltpu.VMEM((kernel, channels), F32),
            pltpu.VMEM((2 * groups, LANES), F32),
            dma((4,)), dma((5,)),
        ],
        compiler_params=pltpu.CompilerParams(vmem_limit_bytes=VMEM_GRANT),
    )(*results)
    return (d_value, d_gate, d_taps, d_gain.reshape(-1), d_shift.reshape(-1))


def solution(mesh):
    return jax.shard_map(
        functools.partial(shards, mesh.shape["sp"]),
        mesh=mesh,
        in_specs=(
            P("sp", "tp"),
            P("sp", "tp"),
            P(None, "tp"),
            P("tp"),
            P("tp"),
            P("tp", None),
            P("sp", None),
        ),
        out_specs=(P("sp", "tp"), P("sp", "tp"), P(None, "tp"), P("tp"), P("tp")),
        check_vma=False,
    )
```

profile of v0, /device:TPU:0, one launch (start us, length us, event | category | flops | bytes accessed | tf_op | source)
XLA Modules:
  0.0 34.7 jit_solution(6893016497893283448)
XLA Ops:
  0.6 32.0 %shard_map.137 = (bf16[256,1024]{1,0:T(8,128)(2,1)}, bf16[256,1024]{1,0:T(8,128)(2,1)}, f32[31,1024]{1,0:T(8,128)}, f32[16,128]{1,0:T(8,128)}) custom-call(bf16[256,1024]{1,0:T(8,128)(2,1)} %value_h.1, bf16[256,1024]{1,0:T(8,128)(2,1)} %gate_h.1, f32[31,1024]{1,0:T(8,128)} %taps_h.1, f32[1,1024]{1,0:T(1,128)} %bitcast.4, f32[1,1024]{1,0:T(1,128)} %bitcast.5, ...), custom_call_target="tpu_custom_call" | custom-call | tf_op jit(solution)/shard_map/pallas_call | solution.py:473
  32.6 2.1 %shard_map.138 = (bf16[256,1024]{1,0:T(8,128)(2,1)}, bf16[256,1024]{1,0:T(8,128)(2,1)}, f32[31,1024]{1,0:T(8,128)}, f32[8,128]{1,0:T(8,128)}, f32[8,128]{1,0:T(8,128)}) custom-call(bf16[256,1024]{1,0:T(8,128)(2,1)} %get-tuple-element.14.refs_0_, bf16[256,1024]{1,0:T(8,128)(2,1)} %get-tuple-element.15.refs_1_, f32[31,1024]{1,0:T(8,128)} %get-tuple-element.16.refs_2_, ...), custom_call_target="tpu_custom_call" | custom-call | tf_op jit(solution)/shard_map/pallas_call | solution.py:527
where the time goes:
time: 34.9 us; the launch traced here: 34.7 us
  Pallas kernels  34.1 us (98%)
  between operations  0.64 us (2%)
    pallas_call x1, Pallas kernels, shards(): pl.pallas_call(functools.partial(body, plan, n, tiles, per, total), out_s...  32 us
    pallas_call x1, Pallas kernels, shards(): pl.pallas_call(store, out_shape=(jax.ShapeDtypeStruct((rows, channels), B...  2.12 us

commit v1 on v0

v1 whole, which is shorter than its diff:
```python
import functools
import math

import jax
import jax.numpy as jnp
import numpy as np
from jax import lax
from jax.experimental import pallas as pl
from jax.experimental.pallas import tpu as pltpu
from jax.sharding import PartitionSpec as P

EPS = 1e-05
ALIGN = 16
LANES = 128
CHUNK = 256
VMEM_GRANT = 48 * 1024 * 1024
F32 = jnp.float32
BF16 = jnp.bfloat16


class Plan:
    def __init__(self, rows, kernel, total):
        self.half = kernel // 2
        self.kernel = kernel
        self.rows = rows
        self.edge = -(-self.half // ALIGN) * ALIGN
        edge = self.edge
        self.block = rows // 2
        self.size = self.block + 2 * edge
        size = self.size
        self.freqs = size // 2
        self.wide = rows + 2 * edge
        omega = 2.0 * np.pi * (np.arange(self.freqs) + 0.5) / size

        def spectrum(times):
            angle = omega[:, None] * times[None, :]
            return np.concatenate([np.cos(angle), np.sin(angle)], 0)

        def inverse(times):
            angle = times[:, None] * omega[None, :]
            return np.concatenate([np.cos(angle), -np.sin(angle)], 1)

        own = np.arange(self.block)
        self.tap_rows = -(-kernel // ALIGN) * ALIGN
        lags = inverse(np.arange(self.tap_rows) - self.half)
        lags[kernel:] = 0.0
        self.mats = np.concatenate(
            [
                spectrum(np.arange(size)),
                inverse(own + edge - self.half),
                inverse(own + edge + self.half),
                lags,
            ],
            0,
        )
        self.at_conv = size
        self.at_grad = self.at_conv + self.block
        self.at_lags = self.at_grad + self.block
        self.own = spectrum(own + edge)
        taps = np.zeros((size, self.tap_rows))
        taps[:, :kernel] = spectrum(np.arange(kernel)) * (2.0 / size)
        high = taps.astype(jnp.bfloat16)
        low = taps - high.astype(np.float64)
        self.taps = np.concatenate([high.astype(np.float64), high.astype(np.float64), low], 1)
        self.lag_scale = 2.0 / size / math.sqrt(total)


class Owners:
    def __init__(self, n, tiles):
        self.count = max(1, min(n // 2, tiles))
        self.per = -(-tiles // self.count)
        self.first = (n - self.count) // 2


def dot(a, b):
    return jnp.dot(a, b, preferred_element_type=F32)


def sigmoid(x):
    return 0.5 * jnp.tanh(0.5 * x) + 0.5


def body(
    plan, n, tiles, owners, total,
    value_h, gate_h, taps_h, gain_h, shift_h, w_h, go_h, mats_h, own_h, ft_h,
    dv, dg, dt_o, dgs_o,
    value, gate, taps, gain, shift, w, go, mats, own, ft,
    sig_s, gw, conv, gm, gcw, tcat, ts, g_spec, acc1, acc2,
    st1, st1_in, st2, st2_in, inv_s, colg, cols,
    gs, rs_src, rs_in, ag,
    load_sem, w_sem, halo_send, halo_recv, tp_send, tp_recv,
    all_send, all_recv,
):
    sp = lax.axis_index("sp")
    tp = lax.axis_index("tp")
    rows, edge, block = plan.rows, plan.edge, plan.block
    channels = value.shape[1]
    width = channels * 2
    chunks = channels // CHUNK
    size, freqs = plan.size, plan.freqs
    per = owners.per
    nxt = lax.rem(sp + 1, n)
    prv = lax.rem(sp + n - 1, n)
    has_prv = sp > 0
    has_nxt = sp < n - 1
    is_owner = (sp >= owners.first) & (sp < owners.first + owners.count)
    low_side = sp < n // 2

    def peer(d):
        return lax.rem(sp + d, n)

    barrier = pltpu.get_barrier_semaphore()

    pairs = [
        (value_h, value), (gate_h, gate), (taps_h, taps), (ft_h, ft), (own_h, own),
        (mats_h, mats), (go_h, go), (gain_h, gain), (shift_h, shift),
    ]
    loads = [
        pltpu.make_async_copy(a, b, load_sem.at[i]) for i, (a, b) in enumerate(pairs)
    ]
    for load in loads:
        load.start()

    def w_copy(c):
        part = pl.ds(pl.multiple_of(c * CHUNK, CHUNK), CHUNK)
        return pltpu.make_async_copy(w_h.at[part], w.at[part], w_sem.at[c])

    for c in range(chunks):
        w_copy(c).start()

    def greet(d, carry):
        pl.semaphore_signal(
            barrier, 1, device_id=(peer(d), tp), device_id_type=pl.DeviceIdType.MESH
        )
        return carry

    pl.semaphore_signal(
        barrier, 1, device_id=(sp, 1 - tp), device_id_type=pl.DeviceIdType.MESH
    )
    lax.fori_loop(1, n, greet, 0)

    def cut(c):
        return pl.ds(c * CHUNK, CHUNK)

    loads[0].wait()
    loads[1].wait()

    def gate_step(i, carry):
        part = pl.ds(pl.multiple_of(i * ALIGN, ALIGN), ALIGN)
        place = pl.ds(pl.multiple_of(i * ALIGN + edge, ALIGN), ALIGN)
        sig = sigmoid(gate[part].astype(F32))
        sig_s[part] = sig
        gw[place] = (value[part].astype(F32) * sig).astype(BF16)
        return carry

    lax.fori_loop(0, rows // ALIGN, gate_step, 0, unroll=4)

    def remote(src, dst, send, recv, device):
        return pltpu.make_async_remote_copy(
            src_ref=src, dst_ref=dst, send_sem=send, recv_sem=recv,
            device_id=device, device_id_type=pl.DeviceIdType.MESH,
        )

    def halo_pair(ref, k):
        return (
            remote(ref.at[pl.ds(rows, edge)], ref.at[pl.ds(0, edge)],
                   halo_send.at[k], halo_recv.at[k], (nxt, tp)),
            remote(ref.at[pl.ds(edge, edge)], ref.at[pl.ds(rows + edge, edge)],
                   halo_send.at[k + 1], halo_recv.at[k + 1], (prv, tp)),
        )

    def send_halo(pair):
        @pl.when(has_nxt)
        def _():
            pair[0].start()

        @pl.when(has_prv)
        def _():
            pair[1].start()

    def recv_prv(pair, ref):
        @pl.when(has_prv)
        def _():
            pair[0].wait_recv()

        @pl.when(sp == 0)
        def _():
            ref[pl.ds(0, edge)] = jnp.zeros((edge, channels), BF16)

    def recv_nxt(pair, ref):
        @pl.when(has_nxt)
        def _():
            pair[1].wait_recv()

        @pl.when(sp == n - 1)
        def _():
            ref[pl.ds(rows + edge, edge)] = jnp.zeros((edge, channels), BF16)

    def sent_halo(pair):
        @pl.when(has_nxt)
        def _():
            pair[0].wait_send()

        @pl.when(has_prv)
        def _():
            pair[1].wait_send()

    gw_halo = halo_pair(gw, 0)
    gc_halo = halo_pair(gcw, 2)

    pl.semaphore_wait(barrier, n)
    send_halo(gw_halo)

    for load in loads[2:7]:
        load.wait()

    tap = jnp.concatenate(
        [taps[...], jnp.zeros((plan.tap_rows - plan.kernel, channels), F32)], 0
    )
    tap_high = tap.astype(BF16)
    tap_low = (tap - tap_high.astype(F32)).astype(BF16)
    for k, part in enumerate((tap_high, tap_low, tap_high)):
        tcat[pl.ds(k * plan.tap_rows, plan.tap_rows)] = part

    def tap_step(_, carry):
        for c in range(chunks):
            ts[:, cut(c)] = dot(ft[...], tcat[:, cut(c)])
        return carry

    lax.fori_loop(0, 1, tap_step, 0)

    def mix(a, b):
        return lax.dot_general(a, b, (((1,), (1,)), ((), ())), preferred_element_type=F32)

    def mix_step(c, carry):
        part = pl.ds(pl.multiple_of(c * CHUNK, CHUNK), CHUNK)
        w_copy(c).wait()
        gm[:, part] = mix(go[...], w[part])
        return carry

    lax.fori_loop(0, chunks, mix_step, 0)

    def fold(x):
        out = x[:, :LANES]
        for k in range(1, x.shape[1] // LANES):
            out = out + x[:, k * LANES : (k + 1) * LANES]
        return out

    first_lanes = lax.broadcasted_iota(jnp.int32, (block, LANES), 1) < LANES // 2

    def conv_step(b):
        place = pl.ds(b * block, block)
        one = two = None
        for c in range(chunks):
            ta = ts[pl.ds(0, freqs), cut(c)]
            tb = ts[pl.ds(freqs, freqs), cut(c)]
            spec = dot(mats[pl.ds(0, size)], gw[pl.ds(b * block, size), cut(c)])
            g_spec[pl.ds(b * size, size), cut(c)] = spec
            re, im = spec[:freqs], spec[freqs:]
            prod = jnp.concatenate([re * ta + im * tb, re * tb - im * ta], 0).astype(BF16)
            out = dot(mats[pl.ds(plan.at_conv, block)], prod)
            conv[place, cut(c)] = out
            if c == 0:
                acc1[...] = fold(out)
                acc2[...] = fold(out * out)
            else:
                acc1[...] += fold(out)
                acc2[...] += fold(out * out)
        st1[place] = jnp.where(
            first_lanes,
            jnp.sum(acc1[...], 1, keepdims=True),
            jnp.sum(acc2[...], 1, keepdims=True),
        )

    def swap(src, dst, b, k):
        place = pl.ds(b * block, block)
        return remote(
            src.at[place], dst.at[place], tp_send.at[k], tp_recv.at[k], (sp, 1 - tp)
        )

    swap1 = [swap(st1, st1_in, b, b) for b in range(2)]
    swap2 = [swap(st2, st2_in, b, 2 + b) for b in range(2)]

    def conv_at(b):
        def step(_, carry):
            conv_step(b)
            return carry

        lax.fori_loop(0, 1, step, 0)

    recv_prv(gw_halo, gw)
    conv_at(0)
    swap1[0].start()
    recv_nxt(gw_halo, gw)
    conv_at(1)
    swap1[1].start()

    loads[7].wait()
    loads[8].wait()
    colg[...] = jnp.zeros_like(colg)
    cols[...] = jnp.zeros_like(cols)
    lanes = lax.broadcasted_iota(jnp.int32, (ALIGN, LANES), 1) < LANES // 2

    def norm_step(i, carry):
        part = pl.ds(pl.multiple_of(i * ALIGN, ALIGN), ALIGN)
        tot = (st1[part] + st1_in[part]) * (1.0 / width)
        mean = tot[:, :1]
        var = tot[:, LANES // 2 : LANES // 2 + 1] - mean * mean
        inv = lax.rsqrt(var + EPS)
        normed = (conv[part] - mean) * inv
        pre = normed * gain[...] + shift[...]
        sig = sigmoid(pre)
        gp = gm[part] * sig * (1.0 + pre * (1.0 - sig))
        gn = gp * gain[...]
        conv[part] = normed
        gm[part] = gn
        gx = gn * normed
        st2[part] = jnp.where(
            lanes,
            jnp.sum(fold(gn), 1, keepdims=True),
            jnp.sum(fold(gx), 1, keepdims=True),
        )
        inv_s[part] = jnp.broadcast_to(inv, (ALIGN, LANES))
        gpn = gp * normed
        colg[...] += gpn[:8] + gpn[8:]
        cols[...] += gp[:8] + gp[8:]
        return carry

    steps = block // ALIGN

    swap1[0].wait_recv()
    lax.fori_loop(0, steps, norm_step, 0, unroll=4)
    swap2[0].start()
    swap1[1].wait_recv()
    lax.fori_loop(steps, 2 * steps, norm_step, 0, unroll=4)
    swap2[1].start()

    rg = jnp.sum(colg[...], 0, keepdims=True)
    rsh = jnp.sum(cols[...], 0, keepdims=True)
    groups = channels // LANES
    gs[sp] = jnp.concatenate(
        [x[:, k * LANES : (k + 1) * LANES] for x in (rg, rsh) for k in range(groups)], 0
    ).astype(BF16)

    def send_gs(d, carry):
        remote(gs.at[sp], gs.at[sp], all_send.at[0], all_recv.at[0], (peer(d), tp)).start()
        return carry

    lax.fori_loop(1, n, send_gs, 0)

    def gc_step(i, carry):
        part = pl.ds(pl.multiple_of(i * ALIGN, ALIGN), ALIGN)
        place = pl.ds(pl.multiple_of(i * ALIGN + edge, ALIGN), ALIGN)
        tot = (st2[part] + st2_in[part]) * (1.0 / width)
        m1 = tot[:, :1]
        m2 = tot[:, LANES // 2 : LANES // 2 + 1]
        inv = inv_s[part][:, :1]
        gcw[place] = (inv * (gm[part] - m1 - conv[part] * m2)).astype(BF16)
        return carry

    swap2[0].wait_recv()
    lax.fori_loop(0, steps, gc_step, 0, unroll=4)
    swap2[1].wait_recv()
    lax.fori_loop(steps, 2 * steps, gc_step, 0, unroll=4)
    send_halo(gc_halo)

    slots = owners.count * per
    if slots > tiles:
        rs_src[pl.ds(tiles, slots - tiles)] = jnp.zeros((slots - tiles, ALIGN, LANES), BF16)

    def spec_step(_, carry):
        for c in range(chunks):
            dr = di = None
            for b in range(2):
                spec = dot(own[...], gcw[pl.ds(edge + b * block, block), cut(c)])
                re, im = spec[:freqs], spec[freqs:]
                hr = g_spec[pl.ds(b * size, freqs), cut(c)]
                hi = g_spec[pl.ds(b * size + freqs, freqs), cut(c)]
                r, i = hr * re + hi * im, hr * im - hi * re
                dr, di = (r, i) if b == 0 else (dr + r, di + i)
            prod = jnp.concatenate([dr, di], 0).astype(BF16)
            out = dot(mats[pl.ds(plan.at_lags, plan.tap_rows)], prod) * plan.lag_scale
            out = out.astype(BF16)
            for r in range(plan.tap_rows // ALIGN):
                for k in range(CHUNK // LANES):
                    rs_src[r * groups + c * (CHUNK // LANES) + k] = out[
                        r * ALIGN : (r + 1) * ALIGN, k * LANES : (k + 1) * LANES
                    ]
        return carry

    lax.fori_loop(0, 1, spec_step, 0)

    def send_rs(i, carry):
        o = jnp.where(low_side, owners.count - 1 - i, i)
        to = owners.first + o

        @pl.when(to != sp)
        def _():
            remote(rs_src.at[pl.ds(o * per, per)], rs_in.at[sp],
                   all_send.at[1], all_recv.at[1], (to, tp)).start()

        return carry

    lax.fori_loop(0, owners.count, send_rs, 0)

    recv_prv(gc_halo, gcw)
    recv_nxt(gc_halo, gcw)

    def out_step(_, carry):
        for c in range(chunks):
            ta = ts[pl.ds(0, freqs), cut(c)]
            tb = ts[pl.ds(freqs, freqs), cut(c)]
            for b in range(2):
                spec = dot(mats[pl.ds(0, size)], gcw[pl.ds(b * block, size), cut(c)])
                re, im = spec[:freqs], spec[freqs:]
                prod = jnp.concatenate([re * ta - im * tb, -(re * tb + im * ta)], 0).astype(BF16)
                out = dot(mats[pl.ds(plan.at_grad, block)], prod)
                place = pl.ds(b * block, block)
                sig = sig_s[place, cut(c)]
                left = out * sig
                dv[place, cut(c)] = left.astype(BF16)
                dg[place, cut(c)] = (
                    left * value[place, cut(c)].astype(F32) * (1.0 - sig)
                ).astype(BF16)
        return carry

    def settle(ref, count, sem):
        if count:
            part = ref.at[pl.ds(0, count)]
            pltpu.make_async_copy(part, part, sem).wait()

    lax.fori_loop(0, 1, out_step, 0)

    @pl.when(is_owner)
    def _():
        o = sp - owners.first
        rs_in[sp] = rs_src[pl.ds(o * per, per)]
        settle(rs_in, n - 1, all_recv.at[1])
        zero = jnp.zeros((per, ALIGN, LANES), F32)
        summed = lax.fori_loop(0, n, lambda i, t: t + rs_in[i].astype(F32), zero)
        ag[o] = summed.astype(BF16)

        def send_ag(i, carry):
            to = jnp.where(low_side, n - 1 - i, i)

            @pl.when(to != sp)
            def _():
                remote(ag.at[o], ag.at[o], all_send.at[2], all_recv.at[2], (to, tp)).start()

            return carry

        lax.fori_loop(0, n, send_ag, 0)

    settle(gs, n - 1, all_recv.at[0])
    small = lax.fori_loop(
        0, n, lambda i, t: t + gs[i].astype(F32), jnp.zeros(gs.shape[1:], F32)
    )
    dgs_o[...] = small * (1.0 / math.sqrt(total))

    sent_halo(gw_halo)
    sent_halo(gc_halo)
    for k in range(2):
        swap1[k].wait_send()
        swap2[k].wait_send()
    settle(gs, n - 1, all_send.at[0])

    @pl.when(is_owner)
    def _():
        settle(rs_in, owners.count - 1, all_send.at[1])
        settle(ag, owners.count - 1, all_recv.at[2])

    @pl.when(jnp.logical_not(is_owner))
    def _():
        settle(rs_in, owners.count, all_send.at[1])
        settle(ag, owners.count, all_recv.at[2])

    for t in range(tiles):
        r, k = t // groups, t % groups
        count = min(ALIGN, plan.kernel - r * ALIGN)
        dt_o[pl.ds(r * ALIGN, count), pl.ds(k * LANES, LANES)] = ag[t // per, t % per].astype(F32)[
            :count
        ]

    @pl.when(is_owner)
    def _():
        def sent(i, carry):
            pltpu.make_async_copy(ag.at[0], ag.at[0], all_send.at[2]).wait()
            return carry

        lax.fori_loop(0, n - 1, sent, 0)


def store(*refs):
    sources, targets, out_sem = refs[:4], refs[4:9], refs[9]
    groups = sources[3].shape[0] // 2
    views = list(sources[:3]) + [
        sources[3].at[pl.ds(0, groups)], sources[3].at[pl.ds(groups, groups)]
    ]
    copies = [
        pltpu.make_async_copy(a, b, out_sem.at[i]) for i, (a, b) in enumerate(zip(views, targets))
    ]
    for copy in copies:
        copy.start()
    for copy in copies:
        copy.wait()


def shards(n, value_in, gate_in, taps, gain, shift, w_out, grad_out):
    rows, channels = value_in.shape
    kernel = taps.shape[0]
    total = rows * n
    plan = Plan(rows, kernel, total)
    groups = channels // LANES
    tiles = plan.tap_rows // ALIGN * groups
    owners = Owners(n, tiles)
    per = owners.per
    model = grad_out.shape[1]
    mats = jnp.asarray(plan.mats, BF16)
    own = jnp.asarray(plan.own, BF16)
    ft = jnp.asarray(plan.taps, BF16)
    hbm = pl.BlockSpec(memory_space=pltpu.HBM)
    vmem = pl.BlockSpec(memory_space=pltpu.VMEM)
    size, block = plan.size, plan.block
    chunks = channels // CHUNK
    dma = pltpu.SemaphoreType.DMA
    results = pl.pallas_call(
        functools.partial(body, plan, n, tiles, owners, total),
        out_shape=(
            pltpu.VMEM((rows, channels), BF16),
            pltpu.VMEM((rows, channels), BF16),
            pltpu.VMEM((kernel, channels), F32),
            pltpu.VMEM((2 * groups, LANES), F32),
        ),
        in_specs=[hbm] * 10,
        out_specs=(vmem,) * 4,
        scratch_shapes=[
            pltpu.VMEM((rows, channels), BF16),
            pltpu.VMEM((rows, channels), BF16),
            pltpu.VMEM((kernel, channels), F32),
            pltpu.VMEM((1, channels), F32),
            pltpu.VMEM((1, channels), F32),
            pltpu.VMEM((channels, model), BF16),
            pltpu.VMEM((rows, model), BF16),
            pltpu.VMEM(plan.mats.shape, BF16),
            pltpu.VMEM(plan.own.shape, BF16),
            pltpu.VMEM(plan.taps.shape, BF16),
            pltpu.VMEM((rows, channels), F32),
            pltpu.VMEM((plan.wide, channels), BF16),
            pltpu.VMEM((rows, channels), F32),
            pltpu.VMEM((rows, channels), F32),
            pltpu.VMEM((plan.wide, channels), BF16),
            pltpu.VMEM((3 * plan.tap_rows, channels), BF16),
            pltpu.VMEM((size, channels), F32),
            pltpu.VMEM((2 * size, channels), F32),
            pltpu.VMEM((block, LANES), F32),
            pltpu.VMEM((block, LANES), F32),
            pltpu.VMEM((rows, LANES), F32),
            pltpu.VMEM((rows, LANES), F32),
            pltpu.VMEM((rows, LANES), F32),
            pltpu.VMEM((rows, LANES), F32),
            pltpu.VMEM((rows, LANES), F32),
            pltpu.VMEM((8, channels), F32),
            pltpu.VMEM((8, channels), F32),
            pltpu.VMEM((n, 2 * groups, LANES), BF16),
            pltpu.VMEM((owners.count * per, ALIGN, LANES), BF16),
            pltpu.VMEM((n, per, ALIGN, LANES), BF16),
            pltpu.VMEM((owners.count, per, ALIGN, LANES), BF16),
            dma((9,)), dma((chunks,)), dma((4,)), dma((4,)),
            dma((4,)), dma((4,)), dma((3,)), dma((3,)),
        ],
        compiler_params=pltpu.CompilerParams(
            collective_id=0, has_side_effects=True, vmem_limit_bytes=VMEM_GRANT
        ),
    )(
        *(
            pltpu.with_memory_space_constraint(x, pltpu.HBM)
            for x in (
                value_in, gate_in, taps, gain.reshape(1, -1), shift.reshape(1, -1), w_out,
                grad_out, mats, own, ft,
            )
        )
    )
    results = [pltpu.with_memory_space_constraint(x, pltpu.VMEM) for x in results]
    d_value, d_gate, d_taps, d_gain, d_shift = pl.pallas_call(
        store,
        out_shape=(
            jax.ShapeDtypeStruct((rows, channels), BF16),
            jax.ShapeDtypeStruct((rows, channels), BF16),
            jax.ShapeDtypeStruct((kernel, channels), F32),
            jax.ShapeDtypeStruct((groups, LANES), F32),
            jax.ShapeDtypeStruct((groups, LANES), F32),
        ),
        in_specs=[vmem] * 4,
        out_specs=(hbm,) * 5,
        scratch_shapes=[dma((5,))],
        compiler_params=pltpu.CompilerParams(vmem_limit_bytes=8 * 1024 * 1024),
    )(*results)
    return (d_value, d_gate, d_taps, d_gain.reshape(-1), d_shift.reshape(-1))


def solution(mesh):
    return jax.shard_map(
        functools.partial(shards, mesh.shape["sp"]),
        mesh=mesh,
        in_specs=(
            P("sp", "tp"),
            P("sp", "tp"),
            P(None, "tp"),
            P("tp"),
            P("tp"),
            P("tp", None),
            P("sp", None),
        ),
        out_specs=(P("sp", "tp"), P("sp", "tp"), P(None, "tp"), P("tp"), P("tp")),
        check_vma=False,
    )
```

time: 34.9 us -> 27.7 us (0.79)
  Pallas kernels: 34.1 us -> 26.9 us
    pallas_call x1, Pallas kernels: 32 us -> 25.9 us  [shards(): pl.pallas_call(functools.partial(body, plan, n, tiles, owners, total), ou...]
    pallas_call x1, Pallas kernels: 2.12 us -> 1.05 us  [shards(): pl.pallas_call(store, out_shape=(jax.ShapeDtypeStruct((rows, channels), B...]
where the time goes in v1:
time: 27.7 us; the launch traced here: 27.6 us
  Pallas kernels  26.9 us (97%)
  between operations  0.64 us (2%)
    pallas_call x1, Pallas kernels, shards(): pl.pallas_call(functools.partial(body, plan, n, tiles, owners, total), ou...  25.9 us
    pallas_call x1, Pallas kernels, shards(): pl.pallas_call(store, out_shape=(jax.ShapeDtypeStruct((rows, channels), B...  1.05 us

profile of v1, /device:TPU:0, one launch (start us, length us, event | category | flops | bytes accessed | tf_op | source)
XLA Modules:
  0.0 27.6 jit_solution(16569585011368478082)
XLA Ops:
  0.6 25.9 %shard_map.137 = (bf16[256,1024]{1,0:T(8,128)(2,1)S(1)}, bf16[256,1024]{1,0:T(8,128)(2,1)S(1)}, f32[31,1024]{1,0:T(8,128)S(1)}, f32[16,128]{1,0:T(8,128)S(1)}) custom-call(bf16[256,1024]{1,0:T(8,128)(2,1)} %value_h.1, bf16[256,1024]{1,0:T(8,128)(2,1)} %gate_h.1, f32[31,1024]{1,0:T(8,128)} %taps_h.1, f32[1,1024]{1,0:T(1,128)} %bitcast.4, f32[1,1024]{1,0:T(1,128)} %bitcast.5, ...), custom_call_target="tpu_custom_call" | custom-call | tf_op jit(solution)/shard_map/pallas_call | solution.py:526
  26.5 1.1 %shard_map.138 = (bf16[256,1024]{1,0:T(8,128)(2,1)}, bf16[256,1024]{1,0:T(8,128)(2,1)}, f32[31,1024]{1,0:T(8,128)}, f32[8,128]{1,0:T(8,128)}, f32[8,128]{1,0:T(8,128)}) custom-call(bf16[256,1024]{1,0:T(8,128)(2,1)S(1)} %get-tuple-element.14.refs_0_, bf16[256,1024]{1,0:T(8,128)(2,1)S(1)} %get-tuple-element.15.refs_1_, ...), custom_call_target="tpu_custom_call" | custom-call | tf_op jit(solution)/shard_map/pallas_call | solution.py:584

commit v2 on v1

--- a/solution.py
+++ b/solution.py
@@ -85,10 +85,10 @@
     value_h, gate_h, taps_h, gain_h, shift_h, w_h, go_h, mats_h, own_h, ft_h,
     dv, dg, dt_o, dgs_o,
     value, gate, taps, gain, shift, w, go, mats, own, ft,
-    sig_s, gw, conv, gm, gcw, tcat, ts, g_spec, acc1, acc2,
+    sig_s, gw, conv, gm, gcw, tcat, ts, g_spec, dsp, acc1, acc2,
     st1, st1_in, st2, st2_in, inv_s, colg, cols,
     gs, rs_src, rs_in, ag,
-    load_sem, w_sem, halo_send, halo_recv, tp_send, tp_recv,
+    meet, load_sem, w_sem, halo_send, halo_recv, tp_send, tp_recv,
     all_send, all_recv,
 ):
     sp = lax.axis_index("sp")
@@ -105,6 +105,10 @@
     has_nxt = sp < n - 1
     is_owner = (sp >= owners.first) & (sp < owners.first + owners.count)
     low_side = sp < n // 2
+    crew = 1 << (max(n, 1).bit_length() // 2)
+    crews = -(-n // crew)
+    head = sp - lax.rem(sp, crew)
+    is_head = (sp == head) & (tp == 1)
 
     def peer(d):
         return lax.rem(sp + d, n)
@@ -128,16 +132,75 @@
     for c in range(chunks):
         w_copy(c).start()
 
-    def greet(d, carry):
-        pl.semaphore_signal(
-            barrier, 1, device_id=(peer(d), tp), device_id_type=pl.DeviceIdType.MESH
-        )
-        return carry
-
-    pl.semaphore_signal(
-        barrier, 1, device_id=(sp, 1 - tp), device_id_type=pl.DeviceIdType.MESH
+    def tell(sem, s, t):
+        pl.semaphore_signal(sem, 1, device_id=(s, t), device_id_type=pl.DeviceIdType.MESH)
+
+    members = 2 * jnp.minimum(crew, n - head)
+
+    def each_member(sem):
+        def step(i, carry):
+            s, t = head + i // 2, lax.rem(i, 2)
+
+            @pl.when((s != sp) | (t != tp))
+            def _():
+                tell(sem, s, t)
+
+            return carry
+
+        lax.fori_loop(0, members, step, 0)
+
+    def each_head(sem):
+        def step(i, carry):
+            @pl.when(i * crew != sp)
+            def _():
+                tell(sem, i * crew, 1)
+
+            return carry
+
+        lax.fori_loop(0, crews, step, 0)
+
+    tell(barrier, sp, 1 - tp)
+
+    @pl.when(has_prv)
+    def _():
+        tell(barrier, prv, tp)
+
+    @pl.when(has_nxt)
+    def _():
+        tell(barrier, nxt, tp)
+
+    @pl.when(is_head)
+    def _():
+        each_member(barrier)
+        each_head(barrier)
+
+    greeted = (
+        1 + has_prv.astype(jnp.int32) + has_nxt.astype(jnp.int32)
+        + jnp.where(is_head, crews - 1, 1)
     )
-    lax.fori_loop(1, n, greet, 0)
+
+    def handshake_up():
+        @pl.when(jnp.logical_not(is_head))
+        def _():
+            tell(meet.at[0], head, 1)
+
+    def handshake_across():
+        @pl.when(is_head)
+        def _():
+            pl.semaphore_wait(meet.at[0], members - 1)
+            each_head(meet.at[1])
+
+    def handshake_down():
+        @pl.when(is_head)
+        def _():
+            if crews > 1:
+                pl.semaphore_wait(meet.at[1], crews - 1)
+            each_member(meet.at[2])
+
+    def handshake_done():
+        @pl.when(jnp.logical_not(is_head))
+        def _():
+            pl.semaphore_wait(meet.at[2], 1)
 
     def cut(c):
         return pl.ds(c * CHUNK, CHUNK)
@@ -205,11 +268,17 @@
         def _():
             pair[1].wait_send()
 
+    def settle(ref, count, sem):
+        if count:
+            part = ref.at[pl.ds(0, count)]
+            pltpu.make_async_copy(part, part, sem).wait()
+
     gw_halo = halo_pair(gw, 0)
     gc_halo = halo_pair(gcw, 2)
 
-    pl.semaphore_wait(barrier, n)
+    pl.semaphore_wait(barrier, greeted)
     send_halo(gw_halo)
+    handshake_up()
 
     for load in loads[2:7]:
         load.wait()
@@ -238,7 +307,9 @@
         gm[:, part] = mix(go[...], w[part])
         return carry
 
-    lax.fori_loop(0, chunks, mix_step, 0)
+    early = chunks - chunks // 4
+    lax.fori_loop(0, early, mix_step, 0)
+    handshake_across()
 
     def fold(x):
         out = x[:, :LANES]
@@ -294,6 +365,8 @@
     recv_nxt(gw_halo, gw)
     conv_at(1)
     swap1[1].start()
+    handshake_down()
+    lax.fori_loop(early, chunks, mix_step, 0)
 
     loads[7].wait()
     loads[8].wait()
@@ -346,6 +419,7 @@
         remote(gs.at[sp], gs.at[sp], all_send.at[0], all_recv.at[0], (peer(d), tp)).start()
         return carry
 
+    handshake_done()
     lax.fori_loop(1, n, send_gs, 0)
 
     def gc_step(i, carry):
@@ -358,40 +432,20 @@
         gcw[place] = (inv * (gm[part] - m1 - conv[part] * m2)).astype(BF16)
         return carry
 
-    swap2[0].wait_recv()
-    lax.fori_loop(0, steps, gc_step, 0, unroll=4)
-    swap2[1].wait_recv()
-    lax.fori_loop(steps, 2 * steps, gc_step, 0, unroll=4)
-    send_halo(gc_halo)
-
     slots = owners.count * per
     if slots > tiles:
         rs_src[pl.ds(tiles, slots - tiles)] = jnp.zeros((slots - tiles, ALIGN, LANES), BF16)
-
-    def spec_step(_, carry):
-        for c in range(chunks):
-            dr = di = None
-            for b in range(2):
-                spec = dot(own[...], gcw[pl.ds(edge + b * block, block), cut(c)])
-                re, im = spec[:freqs], spec[freqs:]
-                hr = g_spec[pl.ds(b * size, freqs), cut(c)]
-                hi = g_spec[pl.ds(b * size + freqs, freqs), cut(c)]
-                r, i = hr * re + hi * im, hr * im - hi * re
-                dr, di = (r, i) if b == 0 else (dr + r, di + i)
-            prod = jnp.concatenate([dr, di], 0).astype(BF16)
-            out = dot(mats[pl.ds(plan.at_lags, plan.tap_rows)], prod) * plan.lag_scale
-            out = out.astype(BF16)
-            for r in range(plan.tap_rows // ALIGN):
-                for k in range(CHUNK // LANES):
-                    rs_src[r * groups + c * (CHUNK // LANES) + k] = out[
-                        r * ALIGN : (r + 1) * ALIGN, k * LANES : (k + 1) * LANES
-                    ]
-        return carry
-
-    lax.fori_loop(0, 1, spec_step, 0)
-
-    def send_rs(i, carry):
-        o = jnp.where(low_side, owners.count - 1 - i, i)
+    tall = plan.tap_rows // ALIGN
+    ready = tall * (CHUNK // LANES)
+
+    def lag_part(b, c):
+        spec = dot(own[...], gcw[pl.ds(edge + b * block, block), cut(c)])
+        re, im = spec[:freqs], spec[freqs:]
+        hr = g_spec[pl.ds(b * size, freqs), cut(c)]
+        hi = g_spec[pl.ds(b * size + freqs, freqs), cut(c)]
+        return hr * re + hi * im, hr * im - hi * re
+
+    def send_rs(o):
         to = owners.first + o
 
         @pl.when(to != sp)
@@ -399,9 +453,64 @@
             remote(rs_src.at[pl.ds(o * per, per)], rs_in.at[sp],
                    all_send.at[1], all_recv.at[1], (to, tp)).start()
 
+    def spec_first(_, carry):
+        for c in range(chunks):
+            dr, di = lag_part(0, c)
+            dsp[pl.ds(0, freqs), cut(c)] = dr
+            dsp[pl.ds(freqs, freqs), cut(c)] = di
         return carry
 
-    lax.fori_loop(0, owners.count, send_rs, 0)
+    def spec_last(c):
+        dr, di = lag_part(1, c)
+        dr = dr + dsp[pl.ds(0, freqs), cut(c)]
+        di = di + dsp[pl.ds(freqs, freqs), cut(c)]
+        prod = jnp.concatenate([dr, di], 0).astype(BF16)
+        out = dot(mats[pl.ds(plan.at_lags, plan.tap_rows)], prod) * plan.lag_scale
+        out = out.astype(BF16)
+        for r in range(tall):
+            for k in range(CHUNK // LANES):
+                rs_src[(c * (CHUNK // LANES) + k) * tall + r] = out[
+                    r * ALIGN : (r + 1) * ALIGN, k * LANES : (k + 1) * LANES
+                ]
+
+    swap2[0].wait_recv()
+    lax.fori_loop(0, steps, gc_step, 0, unroll=4)
+    lax.fori_loop(0, 1, spec_first, 0)
+    swap2[1].wait_recv()
+    lax.fori_loop(steps, 2 * steps, gc_step, 0, unroll=4)
+
+    def spec_phase(c0, count):
+        for c in range(c0, c0 + count):
+            spec_last(c)
+        for o in range(owners.count):
+            last = (min((o + 1) * per, tiles) - 1) // ready
+            if c0 <= last < c0 + count:
+                send_rs(o)
+
+    group = 2 if chunks % 2 == 0 else 1
+    for c0 in range(0, chunks, group):
+        spec_phase(c0, group)
+    send_halo(gc_halo)
+
+    @pl.when(is_owner)
+    def _():
+        o = sp - owners.first
+        rs_in[sp] = rs_src[pl.ds(o * per, per)]
+        settle(rs_in, n - 1, all_recv.at[1])
+        zero = jnp.zeros((per, ALIGN, LANES), F32)
+        summed = lax.fori_loop(0, n, lambda i, t: t + rs_in[i].astype(F32), zero)
+        ag[o] = summed.astype(BF16)
+
+        def send_ag(i, carry):
+            to = jnp.where(low_side, n - 1 - i, i)
+
+            @pl.when(to != sp)
+            def _():
+                remote(ag.at[o], ag.at[o], all_send.at[2], all_recv.at[2], (to, tp)).start()
+
+            return carry
+
+        lax.fori_loop(0, n, send_ag, 0)
 
     recv_prv(gc_halo, gcw)
     recv_nxt(gc_halo, gcw)
@@ -424,32 +533,7 @@
                 ).astype(BF16)
         return carry
 
-    def settle(ref, count, sem):
-        if count:
-            part = ref.at[pl.ds(0, count)]
-            pltpu.make_async_copy(part, part, sem).wait()
-
     lax.fori_loop(0, 1, out_step, 0)
-
-    @pl.when(is_owner)
-    def _():
-        o = sp - owners.first
-        rs_in[sp] = rs_src[pl.ds(o * per, per)]
-        settle(rs_in, n - 1, all_recv.at[1])
-        zero = jnp.zeros((per, ALIGN, LANES), F32)
-        summed = lax.fori_loop(0, n, lambda i, t: t + rs_in[i].astype(F32), zero)
-        ag[o] = summed.astype(BF16)
-
-        def send_ag(i, carry):
-            to = jnp.where(low_side, n - 1 - i, i)
-
-            @pl.when(to != sp)
-            def _():
-                remote(ag.at[o], ag.at[o], all_send.at[2], all_recv.at[2], (to, tp)).start()
-
-            return carry
-
-        lax.fori_loop(0, n, send_ag, 0)
 
     settle(gs, n - 1, all_recv.at[0])
     small = lax.fori_loop(
@@ -475,7 +559,7 @@
         settle(ag, owners.count, all_recv.at[2])
 
     for t in range(tiles):
-        r, k = t // groups, t % groups
+        k, r = t // tall, t % tall
         count = min(ALIGN, plan.kernel - r * ALIGN)
         dt_o[pl.ds(r * ALIGN, count), pl.ds(k * LANES, LANES)] = ag[t // per, t % per].astype(F32)[
             :count
@@ -552,6 +636,7 @@
             pltpu.VMEM((3 * plan.tap_rows, channels), BF16),
             pltpu.VMEM((size, channels), F32),
             pltpu.VMEM((2 * size, channels), F32),
+            pltpu.VMEM((size, channels), F32),
             pltpu.VMEM((block, LANES), F32),
             pltpu.VMEM((block, LANES), F32),
             pltpu.VMEM((rows, LANES), F32),
@@ -565,6 +650,7 @@
             pltpu.VMEM((owners.count * per, ALIGN, LANES), BF16),
             pltpu.VMEM((n, per, ALIGN, LANES), BF16),
             pltpu.VMEM((owners.count, per, ALIGN, LANES), BF16),
+            pltpu.SemaphoreType.REGULAR((3,)),
             dma((9,)), dma((chunks,)), dma((4,)), dma((4,)),
             dma((4,)), dma((4,)), dma((3,)), dma((3,)),
         ],

time: 27.7 us -> 26 us (0.939)
  Pallas kernels: 26.9 us -> 25.2 us
    pallas_call x1, Pallas kernels: 25.9 us -> 24.1 us  [shards(): pl.pallas_call(functools.partial(body, plan, n, tiles, owners, total), ou...]
where the time goes in v2:
time: 26 us; the launch traced here: 25.8 us
  Pallas kernels  25.2 us (97%)
  between operations  0.64 us (2%)
    pallas_call x1, Pallas kernels, shards(): pl.pallas_call(functools.partial(body, plan, n, tiles, owners, total), ou...  24.1 us
    pallas_call x1, Pallas kernels, shards(): pl.pallas_call(store, out_shape=(jax.ShapeDtypeStruct((rows, channels), B...  1.05 us

profile of v2, /device:TPU:0, one launch (start us, length us, event | category | flops | bytes accessed | tf_op | source)
XLA Modules:
  0.0 25.8 jit_solution(9837820856853118747)
XLA Ops:
  0.6 24.1 %shard_map.137 = (bf16[256,1024]{1,0:T(8,128)(2,1)S(1)}, bf16[256,1024]{1,0:T(8,128)(2,1)S(1)}, f32[31,1024]{1,0:T(8,128)S(1)}, f32[16,128]{1,0:T(8,128)S(1)}) custom-call(bf16[256,1024]{1,0:T(8,128)(2,1)} %value_h.1, bf16[256,1024]{1,0:T(8,128)(2,1)} %gate_h.1, f32[31,1024]{1,0:T(8,128)} %taps_h.1, f32[1,1024]{1,0:T(1,128)} %bitcast.4, f32[1,1024]{1,0:T(1,128)} %bitcast.5, ...), custom_call_target="tpu_custom_call" | custom-call | tf_op jit(solution)/shard_map/pallas_call | solution.py:610
  24.8 1.1 %shard_map.138 = (bf16[256,1024]{1,0:T(8,128)(2,1)}, bf16[256,1024]{1,0:T(8,128)(2,1)}, f32[31,1024]{1,0:T(8,128)}, f32[8,128]{1,0:T(8,128)}, f32[8,128]{1,0:T(8,128)}) custom-call(bf16[256,1024]{1,0:T(8,128)(2,1)S(1)} %get-tuple-element.14.refs_0_, bf16[256,1024]{1,0:T(8,128)(2,1)S(1)} %get-tuple-element.15.refs_1_, ...), custom_call_target="tpu_custom_call" | custom-call | tf_op jit(solution)/shard_map/pallas_call | solution.py:670

commit v3 on v2

--- a/solution.py
+++ b/solution.py
@@ -84,10 +84,10 @@
     plan, n, tiles, owners, total,
     value_h, gate_h, taps_h, gain_h, shift_h, w_h, go_h, mats_h, own_h, ft_h,
     dv, dg, dt_o, dgs_o,
-    value, gate, taps, gain, shift, w, go, mats, own, ft,
-    sig_s, gw, conv, gm, gcw, tcat, ts, g_spec, dsp, acc1, acc2,
-    st1, st1_in, st2, st2_in, inv_s, colg, cols,
-    gs, rs_src, rs_in, ag,
+    value, gate, taps, w, go, mats,
+    sig_s, gw, conv, gm, gcw, tcat, ts, g_spec, spec_s, dsp, prod,
+    st1, st1_in, st2, st2_in, inv_s, colg, cols, hgain, hshift,
+    gs, rs_src, rs_in, ag, own, ft, gain, shift,
     meet, load_sem, w_sem, halo_send, halo_recv, tp_send, tp_recv,
     all_send, all_recv,
 ):
@@ -317,31 +317,33 @@
             out = out + x[:, k * LANES : (k + 1) * LANES]
         return out
 
-    first_lanes = lax.broadcasted_iota(jnp.int32, (block, LANES), 1) < LANES // 2
+    lanes = lax.broadcasted_iota(jnp.int32, (ALIGN, LANES), 1) < LANES // 2
+
+    def multiply(spec, sign):
+        for f in range(0, freqs, ALIGN):
+            high, low = pl.ds(f, ALIGN), pl.ds(freqs + f, ALIGN)
+            for c in range(chunks):
+                re, im = spec[high, cut(c)], spec[low, cut(c)]
+                ta, tb = ts[high, cut(c)], ts[low, cut(c)]
+                prod[high, cut(c)] = (re * ta + sign * im * tb).astype(BF16)
+                other = re * tb - sign * im * ta
+                prod[low, cut(c)] = (sign * other).astype(BF16)
 
     def conv_step(b):
-        place = pl.ds(b * block, block)
-        one = two = None
-        for c in range(chunks):
-            ta = ts[pl.ds(0, freqs), cut(c)]
-            tb = ts[pl.ds(freqs, freqs), cut(c)]
-            spec = dot(mats[pl.ds(0, size)], gw[pl.ds(b * block, size), cut(c)])
-            g_spec[pl.ds(b * size, size), cut(c)] = spec
-            re, im = spec[:freqs], spec[freqs:]
-            prod = jnp.concatenate([re * ta + im * tb, re * tb - im * ta], 0).astype(BF16)
-            out = dot(mats[pl.ds(plan.at_conv, block)], prod)
-            conv[place, cut(c)] = out
-            if c == 0:
-                acc1[...] = fold(out)
-                acc2[...] = fold(out * out)
-            else:
-                acc1[...] += fold(out)
-                acc2[...] += fold(out * out)
-        st1[place] = jnp.where(
-            first_lanes,
-            jnp.sum(acc1[...], 1, keepdims=True),
-            jnp.sum(acc2[...], 1, keepdims=True),
-        )
+        start = b * block
+        spec = g_spec.at[pl.ds(b * size, size)]
+        spec[...] = dot(mats[pl.ds(0, size)], gw[pl.ds(start, size)])
+        multiply(spec, 1.0)
+        conv[pl.ds(start, block)] = dot(mats[pl.ds(plan.at_conv, block)], prod[...])
+        for r in range(start, start + block, ALIGN):
+            one = two = None
+            for c in range(chunks):
+                x = conv[pl.ds(r, ALIGN), cut(c)]
+                p, q = fold(x), fold(x * x)
+                one, two = (p, q) if c == 0 else (one + p, two + q)
+            st1[pl.ds(r, ALIGN)] = jnp.where(
+                lanes, jnp.sum(one, 1, keepdims=True), jnp.sum(two, 1, keepdims=True)
+            )
 
     def swap(src, dst, b, k):
         place = pl.ds(b * block, block)
@@ -370,42 +372,57 @@
 
     loads[7].wait()
     loads[8].wait()
-    colg[...] = jnp.zeros_like(colg)
-    cols[...] = jnp.zeros_like(cols)
-    lanes = lax.broadcasted_iota(jnp.int32, (ALIGN, LANES), 1) < LANES // 2
-
-    def norm_step(i, carry):
-        part = pl.ds(pl.multiple_of(i * ALIGN, ALIGN), ALIGN)
-        tot = (st1[part] + st1_in[part]) * (1.0 / width)
-        mean = tot[:, :1]
-        var = tot[:, LANES // 2 : LANES // 2 + 1] - mean * mean
-        inv = lax.rsqrt(var + EPS)
-        normed = (conv[part] - mean) * inv
-        pre = normed * gain[...] + shift[...]
-        sig = sigmoid(pre)
-        gp = gm[part] * sig * (1.0 + pre * (1.0 - sig))
-        gn = gp * gain[...]
-        conv[part] = normed
-        gm[part] = gn
-        gx = gn * normed
-        st2[part] = jnp.where(
-            lanes,
-            jnp.sum(fold(gn), 1, keepdims=True),
-            jnp.sum(fold(gx), 1, keepdims=True),
-        )
-        inv_s[part] = jnp.broadcast_to(inv, (ALIGN, LANES))
-        gpn = gp * normed
-        colg[...] += gpn[:8] + gpn[8:]
-        cols[...] += gp[:8] + gp[8:]
-        return carry
-
-    steps = block // ALIGN
+    hgain[...] = jnp.broadcast_to(0.5 * gain[...], hgain.shape)
+    hshift[...] = jnp.broadcast_to(0.5 * shift[...], hshift.shape)
+
+    def twice(x):
+        return jnp.concatenate([x, x], 0)
+
+    def halves(x):
+        return x[:8] + x[8:]
+
+    def norm_at(b):
+        total_g, total_s = [None] * chunks, [None] * chunks
+        for r in range(b * block, (b + 1) * block, ALIGN):
+            part = pl.ds(r, ALIGN)
+            tot = (st1[part] + st1_in[part]) * (1.0 / width)
+            mean = tot[:, :1]
+            var = tot[:, LANES // 2 : LANES // 2 + 1] - mean * mean
+            inv = lax.rsqrt(var + EPS)
+            inv_s[part] = jnp.broadcast_to(inv, (ALIGN, LANES))
+            one = two = None
+            for c in range(chunks):
+                hg = twice(hgain[:, cut(c)])
+                normed = (conv[part, cut(c)] - mean) * inv
+                half_pre = normed * hg + twice(hshift[:, cut(c)])
+                th = jnp.tanh(half_pre)
+                gp = gm[part, cut(c)] * (1.0 + th) * (1.0 + half_pre * (1.0 - th))
+                gn = gp * hg
+                gpn = gp * normed
+                conv[part, cut(c)] = normed
+                gm[part, cut(c)] = gn
+                p, q = fold(gn), fold(gpn * hg)
+                one, two = (p, q) if c == 0 else (one + p, two + q)
+                g, h = halves(gpn), halves(gp)
+                if total_g[c] is not None:
+                    g, h = total_g[c] + g, total_s[c] + h
+                total_g[c], total_s[c] = g, h
+            st2[part] = jnp.where(
+                lanes, jnp.sum(one, 1, keepdims=True), jnp.sum(two, 1, keepdims=True)
+            )
+        for c in range(chunks):
+            if b == 0:
+                colg[:, cut(c)] = total_g[c]
+                cols[:, cut(c)] = total_s[c]
+            else:
+                colg[:, cut(c)] += total_g[c]
+                cols[:, cut(c)] += total_s[c]
 
     swap1[0].wait_recv()
-    lax.fori_loop(0, steps, norm_step, 0, unroll=4)
+    norm_at(0)
     swap2[0].start()
     swap1[1].wait_recv()
-    lax.fori_loop(steps, 2 * steps, norm_step, 0, unroll=4)
+    norm_at(1)
     swap2[1].start()
 
     rg = jnp.sum(colg[...], 0, keepdims=True)
@@ -422,30 +439,34 @@
     handshake_done()
     lax.fori_loop(1, n, send_gs, 0)
 
-    def gc_step(i, carry):
-        part = pl.ds(pl.multiple_of(i * ALIGN, ALIGN), ALIGN)
-        place = pl.ds(pl.multiple_of(i * ALIGN + edge, ALIGN), ALIGN)
-        tot = (st2[part] + st2_in[part]) * (1.0 / width)
-        m1 = tot[:, :1]
-        m2 = tot[:, LANES // 2 : LANES // 2 + 1]
-        inv = inv_s[part][:, :1]
-        gcw[place] = (inv * (gm[part] - m1 - conv[part] * m2)).astype(BF16)
-        return carry
+    def gc_at(b):
+        for r in range(b * block, (b + 1) * block, ALIGN):
+            part = pl.ds(r, ALIGN)
+            tot = (st2[part] + st2_in[part]) * (1.0 / width)
+            inv = inv_s[part]
+            scaled = inv * tot
+            m1 = scaled[:, :1]
+            m2 = scaled[:, LANES // 2 : LANES // 2 + 1]
+            inv = inv[:, :1]
+            for c in range(chunks):
+                gcw[pl.ds(r + edge, ALIGN), cut(c)] = (
+                    inv * gm[part, cut(c)] - m1 - conv[part, cut(c)] * m2
+                ).astype(BF16)
 
     slots = owners.count * per
     if slots > tiles:
         rs_src[pl.ds(tiles, slots - tiles)] = jnp.zeros((slots - tiles, ALIGN, LANES), BF16)
     tall = plan.tap_rows // ALIGN
-    ready = tall * (CHUNK // LANES)
-
-    def lag_part(b, c):
-        spec = dot(own[...], gcw[pl.ds(edge + b * block, block), cut(c)])
-        re, im = spec[:freqs], spec[freqs:]
-        hr = g_spec[pl.ds(b * size, freqs), cut(c)]
-        hi = g_spec[pl.ds(b * size + freqs, freqs), cut(c)]
-        return hr * re + hi * im, hr * im - hi * re
-
-    def send_rs(o):
+
+    def lag_part(b, f, c):
+        high, low = pl.ds(f, ALIGN), pl.ds(freqs + f, ALIGN)
+        re, im = spec_s[high, cut(c)], spec_s[low, cut(c)]
+        hr = g_spec[pl.ds(b * size + f, ALIGN), cut(c)]
+        hi = g_spec[pl.ds(b * size + freqs + f, ALIGN), cut(c)]
+        return high, low, hr * re + hi * im, hr * im - hi * re
+
+    def send_rs(i, carry):
+        o = jnp.where(low_side, owners.count - 1 - i, i)
         to = owners.first + o
 
         @pl.when(to != sp)
@@ -453,43 +474,41 @@
             remote(rs_src.at[pl.ds(o * per, per)], rs_in.at[sp],
                    all_send.at[1], all_recv.at[1], (to, tp)).start()
 
+        return carry
+
     def spec_first(_, carry):
-        for c in range(chunks):
-            dr, di = lag_part(0, c)
-            dsp[pl.ds(0, freqs), cut(c)] = dr
-            dsp[pl.ds(freqs, freqs), cut(c)] = di
+        spec_s[...] = dot(own[...], gcw[pl.ds(edge, block)])
+        for f in range(0, freqs, ALIGN):
+            for c in range(chunks):
+                high, low, dr, di = lag_part(0, f, c)
+                dsp[high, cut(c)] = dr
+                dsp[low, cut(c)] = di
         return carry
 
-    def spec_last(c):
-        dr, di = lag_part(1, c)
-        dr = dr + dsp[pl.ds(0, freqs), cut(c)]
-        di = di + dsp[pl.ds(freqs, freqs), cut(c)]
-        prod = jnp.concatenate([dr, di], 0).astype(BF16)
-        out = dot(mats[pl.ds(plan.at_lags, plan.tap_rows)], prod) * plan.lag_scale
+    def spec_last(_, carry):
+        spec_s[...] = dot(own[...], gcw[pl.ds(edge + block, block)])
+        for f in range(0, freqs, ALIGN):
+            for c in range(chunks):
+                high, low, dr, di = lag_part(1, f, c)
+                prod[high, cut(c)] = (dr + dsp[high, cut(c)]).astype(BF16)
+                prod[low, cut(c)] = (di + dsp[low, cut(c)]).astype(BF16)
+        out = dot(mats[pl.ds(plan.at_lags, plan.tap_rows)], prod[...]) * plan.lag_scale
         out = out.astype(BF16)
         for r in range(tall):
-            for k in range(CHUNK // LANES):
-                rs_src[(c * (CHUNK // LANES) + k) * tall + r] = out[
+            for k in range(groups):
+                rs_src[k * tall + r] = out[
                     r * ALIGN : (r + 1) * ALIGN, k * LANES : (k + 1) * LANES
                 ]
+        return carry
 
     swap2[0].wait_recv()
-    lax.fori_loop(0, steps, gc_step, 0, unroll=4)
+    gc_at(0)
     lax.fori_loop(0, 1, spec_first, 0)
     swap2[1].wait_recv()
-    lax.fori_loop(steps, 2 * steps, gc_step, 0, unroll=4)
-
-    def spec_phase(c0, count):
-        for c in range(c0, c0 + count):
-            spec_last(c)
-        for o in range(owners.count):
-            last = (min((o + 1) * per, tiles) - 1) // ready
-            if c0 <= last < c0 + count:
-                send_rs(o)
-
-    group = 2 if chunks % 2 == 0 else 1
-    for c0 in range(0, chunks, group):
-        spec_phase(c0, group)
+    gc_at(1)
+
+    lax.fori_loop(0, 1, spec_last, 0)
+    lax.fori_loop(0, owners.count, send_rs, 0)
     send_halo(gc_halo)
 
     @pl.when(is_owner)
@@ -512,34 +531,39 @@
 
         lax.fori_loop(0, n, send_ag, 0)
 
+
+    def out_step(b):
+        start = b * block
+        spec_s[...] = dot(mats[pl.ds(0, size)], gcw[pl.ds(start, size)])
+        multiply(spec_s, -1.0)
+        conv[pl.ds(start, block)] = dot(mats[pl.ds(plan.at_grad, block)], prod[...])
+        for r in range(start, start + block, ALIGN):
+            part = pl.ds(r, ALIGN)
+            for c in range(chunks):
+                sig = sig_s[part, cut(c)]
+                left = conv[part, cut(c)] * sig
+                dv[part, cut(c)] = left.astype(BF16)
+                dg[part, cut(c)] = (
+                    left * value[part, cut(c)].astype(F32) * (1.0 - sig)
+                ).astype(BF16)
+
+    def out_at(b):
+        def step(_, carry):
+            out_step(b)
+            return carry
+
+        lax.fori_loop(0, 1, step, 0)
+
     recv_prv(gc_halo, gcw)
+    out_at(0)
     recv_nxt(gc_halo, gcw)
-
-    def out_step(_, carry):
-        for c in range(chunks):
-            ta = ts[pl.ds(0, freqs), cut(c)]
-            tb = ts[pl.ds(freqs, freqs), cut(c)]
-            for b in range(2):
-                spec = dot(mats[pl.ds(0, size)], gcw[pl.ds(b * block, size), cut(c)])
-                re, im = spec[:freqs], spec[freqs:]
-                prod = jnp.concatenate([re * ta - im * tb, -(re * tb + im * ta)], 0).astype(BF16)
-                out = dot(mats[pl.ds(plan.at_grad, block)], prod)
-                place = pl.ds(b * block, block)
-                sig = sig_s[place, cut(c)]
-                left = out * sig
-                dv[place, cut(c)] = left.astype(BF16)
-                dg[place, cut(c)] = (
-                    left * value[place, cut(c)].astype(F32) * (1.0 - sig)
-                ).astype(BF16)
-        return carry
-
-    lax.fori_loop(0, 1, out_step, 0)
+    out_at(1)
 
     settle(gs, n - 1, all_recv.at[0])
     small = lax.fori_loop(
         0, n, lambda i, t: t + gs[i].astype(F32), jnp.zeros(gs.shape[1:], F32)
     )
-    dgs_o[...] = small * (1.0 / math.sqrt(total))
+    dgs_o[...] = small * (0.5 / math.sqrt(total))
 
     sent_halo(gw_halo)
     sent_halo(gc_halo)
@@ -621,13 +645,9 @@
             pltpu.VMEM((rows, channels), BF16),
             pltpu.VMEM((rows, channels), BF16),
             pltpu.VMEM((kernel, channels), F32),
-            pltpu.VMEM((1, channels), F32),
-            pltpu.VMEM((1, channels), F32),
             pltpu.VMEM((channels, model), BF16),
             pltpu.VMEM((rows, model), BF16),
             pltpu.VMEM(plan.mats.shape, BF16),
-            pltpu.VMEM(plan.own.shape, BF16),
-            pltpu.VMEM(plan.taps.shape, BF16),
             pltpu.VMEM((rows, channels), F32),
             pltpu.VMEM((plan.wide, channels), BF16),
             pltpu.VMEM((rows, channels), F32),
@@ -637,8 +657,8 @@
             pltpu.VMEM((size, channels), F32),
             pltpu.VMEM((2 * size, channels), F32),
             pltpu.VMEM((size, channels), F32),
-            pltpu.VMEM((block, LANES), F32),
-            pltpu.VMEM((block, LANES), F32),
+            pltpu.VMEM((size, channels), F32),
+            pltpu.VMEM((size, channels), BF16),
             pltpu.VMEM((rows, LANES), F32),
             pltpu.VMEM((rows, LANES), F32),
             pltpu.VMEM((rows, LANES), F32),
@@ -646,10 +666,16 @@
             pltpu.VMEM((rows, LANES), F32),
             pltpu.VMEM((8, channels), F32),
             pltpu.VMEM((8, channels), F32),
+            pltpu.VMEM((8, channels), F32),
+            pltpu.VMEM((8, channels), F32),
             pltpu.VMEM((n, 2 * groups, LANES), BF16),
             pltpu.VMEM((owners.count * per, ALIGN, LANES), BF16),
             pltpu.VMEM((n, per, ALIGN, LANES), BF16),
             pltpu.VMEM((owners.count, per, ALIGN, LANES), BF16),
+            pltpu.VMEM(plan.own.shape, BF16),
+            pltpu.VMEM(plan.taps.shape, BF16),
+            pltpu.VMEM((1, channels), F32),
+            pltpu.VMEM((1, channels), F32),
             pltpu.SemaphoreType.REGULAR((3,)),
             dma((9,)), dma((chunks,)), dma((4,)), dma((4,)),
             dma((4,)), dma((4,)), dma((3,)), dma((3,)),

time: 26 us -> 24.2 us (0.931)
  Pallas kernels: 25.2 us -> 23.4 us
    pallas_call x1, Pallas kernels: 24.1 us -> 22.4 us  [shards(): pl.pallas_call(functools.partial(body, plan, n, tiles, owners, total), ou...]
where the time goes in v3:
time: 24.2 us; the launch traced here: 24.1 us
  Pallas kernels  23.4 us (97%)
  between operations  0.64 us (3%)
    pallas_call x1, Pallas kernels, shards(): pl.pallas_call(functools.partial(body, plan, n, tiles, owners, total), ou...  22.4 us
    pallas_call x1, Pallas kernels, shards(): pl.pallas_call(store, out_shape=(jax.ShapeDtypeStruct((rows, channels), B...  1.05 us

profile of v3, /device:TPU:0, one launch (start us, length us, event | category | flops | bytes accessed | tf_op | source)
XLA Modules:
  0.0 24.1 jit_solution(16010485279499017572)
XLA Ops:
  0.6 22.4 %shard_map.137 = (bf16[256,1024]{1,0:T(8,128)(2,1)S(1)}, bf16[256,1024]{1,0:T(8,128)(2,1)S(1)}, f32[31,1024]{1,0:T(8,128)S(1)}, f32[16,128]{1,0:T(8,128)S(1)}) custom-call(bf16[256,1024]{1,0:T(8,128)(2,1)} %value_h.1, bf16[256,1024]{1,0:T(8,128)(2,1)} %gate_h.1, f32[31,1024]{1,0:T(8,128)} %taps_h.1, f32[1,1024]{1,0:T(1,128)} %bitcast.4, f32[1,1024]{1,0:T(1,128)} %bitcast.5, ...), custom_call_target="tpu_custom_call" | custom-call | tf_op jit(solution)/shard_map/pallas_call | solution.py:634
  23.0 1.1 %shard_map.138 = (bf16[256,1024]{1,0:T(8,128)(2,1)}, bf16[256,1024]{1,0:T(8,128)(2,1)}, f32[31,1024]{1,0:T(8,128)}, f32[8,128]{1,0:T(8,128)}, f32[8,128]{1,0:T(8,128)}) custom-call(bf16[256,1024]{1,0:T(8,128)(2,1)S(1)} %get-tuple-element.14.refs_0_, bf16[256,1024]{1,0:T(8,128)(2,1)S(1)} %get-tuple-element.15.refs_1_, ...), custom_call_target="tpu_custom_call" | custom-call | tf_op jit(solution)/shard_map/pallas_call | solution.py:696

commit v4 on v3

--- a/solution.py
+++ b/solution.py
@@ -87,7 +87,7 @@
     value, gate, taps, w, go, mats,
     sig_s, gw, conv, gm, gcw, tcat, ts, g_spec, spec_s, dsp, prod,
     st1, st1_in, st2, st2_in, inv_s, colg, cols, hgain, hshift,
-    gs, rs_src, rs_in, ag, own, ft, gain, shift,
+    gs, rs_src, rs_in, ag_src, ag, own, ft, gain, shift,
     meet, load_sem, w_sem, halo_send, halo_recv, tp_send, tp_recv,
     all_send, all_recv,
 ):
@@ -103,7 +103,7 @@
     prv = lax.rem(sp + n - 1, n)
     has_prv = sp > 0
     has_nxt = sp < n - 1
-    is_owner = (sp >= owners.first) & (sp < owners.first + owners.count)
+    is_owner = (sp >= owners.first) & (sp < owners.first + owners.count) & (tp == 1)
     low_side = sp < n // 2
     crew = 1 << (max(n, 1).bit_length() // 2)
     crews = -(-n // crew)
@@ -115,22 +115,26 @@
 
     barrier = pltpu.get_barrier_semaphore()
 
-    pairs = [
-        (value_h, value), (gate_h, gate), (taps_h, taps), (ft_h, ft), (own_h, own),
-        (mats_h, mats), (go_h, go), (gain_h, gain), (shift_h, shift),
+    inner = pl.ds(edge, rows - 2 * edge)
+    sides = [pl.ds(0, edge), pl.ds(rows - edge, edge)]
+    pairs = [(h.at[part], v.at[part]) for h, v in ((value_h, value), (gate_h, gate)) for part in sides]
+    pairs += [(h.at[inner], v.at[inner]) for h, v in ((value_h, value), (gate_h, gate))]
+    pairs += [(taps_h, taps), (ft_h, ft), (go_h, go)]
+    late = [(mats_h, mats), (own_h, own), (gain_h, gain), (shift_h, shift)]
+    loads = [
+        pltpu.make_async_copy(a, b, load_sem.at[i]) for i, (a, b) in enumerate(pairs + late)
     ]
-    loads = [
-        pltpu.make_async_copy(a, b, load_sem.at[i]) for i, (a, b) in enumerate(pairs)
-    ]
-    for load in loads:
-        load.start()
 
     def w_copy(c):
         part = pl.ds(pl.multiple_of(c * CHUNK, CHUNK), CHUNK)
         return pltpu.make_async_copy(w_h.at[part], w.at[part], w_sem.at[c])
 
+    for load in loads[: len(pairs)]:
+        load.start()
     for c in range(chunks):
         w_copy(c).start()
+    for load in loads[len(pairs):]:
+        load.start()
 
     def tell(sem, s, t):
         pl.semaphore_signal(sem, 1, device_id=(s, t), device_id_type=pl.DeviceIdType.MESH)
@@ -204,9 +208,6 @@
 
     def cut(c):
         return pl.ds(c * CHUNK, CHUNK)
-
-    loads[0].wait()
-    loads[1].wait()
 
     def gate_step(i, carry):
         part = pl.ds(pl.multiple_of(i * ALIGN, ALIGN), ALIGN)
@@ -216,8 +217,6 @@
         gw[place] = (value[part].astype(F32) * sig).astype(BF16)
         return carry
 
-    lax.fori_loop(0, rows // ALIGN, gate_step, 0, unroll=4)
-
     def remote(src, dst, send, recv, device):
         return pltpu.make_async_remote_copy(
             src_ref=src, dst_ref=dst, send_sem=send, recv_sem=recv,
@@ -276,12 +275,20 @@
     gw_halo = halo_pair(gw, 0)
     gc_halo = halo_pair(gcw, 2)
 
+    for load in loads[:4]:
+        load.wait()
+    sided = edge // ALIGN
+    for r in range(sided):
+        gate_step(r, 0)
+        gate_step(rows // ALIGN - 1 - r, 0)
     pl.semaphore_wait(barrier, greeted)
     send_halo(gw_halo)
     handshake_up()
-
-    for load in loads[2:7]:
-        load.wait()
+    loads[4].wait()
+    loads[5].wait()
+    lax.fori_loop(sided, rows // ALIGN - sided, gate_step, 0, unroll=7)
+    loads[6].wait()
+    loads[7].wait()
 
     tap = jnp.concatenate(
         [taps[...], jnp.zeros((plan.tap_rows - plan.kernel, channels), F32)], 0
@@ -307,9 +314,10 @@
         gm[:, part] = mix(go[...], w[part])
         return carry
 
-    early = chunks - chunks // 4
-    lax.fori_loop(0, early, mix_step, 0)
+    loads[8].wait()
+    lax.fori_loop(0, chunks, mix_step, 0)
     handshake_across()
+    loads[9].wait()
 
     def fold(x):
         out = x[:, :LANES]
@@ -368,10 +376,8 @@
     conv_at(1)
     swap1[1].start()
     handshake_down()
-    lax.fori_loop(early, chunks, mix_step, 0)
-
-    loads[7].wait()
-    loads[8].wait()
+    for load in loads[10:]:
+        load.wait()
     hgain[...] = jnp.broadcast_to(0.5 * gain[...], hgain.shape)
     hshift[...] = jnp.broadcast_to(0.5 * shift[...], hshift.shape)
 
@@ -469,10 +475,10 @@
         o = jnp.where(low_side, owners.count - 1 - i, i)
         to = owners.first + o
 
-        @pl.when(to != sp)
-        def _():
-            remote(rs_src.at[pl.ds(o * per, per)], rs_in.at[sp],
-                   all_send.at[1], all_recv.at[1], (to, tp)).start()
+        @pl.when((to != sp) | (tp != 1))
+        def _():
+            remote(rs_src.at[pl.ds(o * per, per)], rs_in.at[2 * sp + tp],
+                   all_send.at[1], all_recv.at[1], (to, 1)).start()
 
         return carry
 
@@ -514,23 +520,25 @@
     @pl.when(is_owner)
     def _():
         o = sp - owners.first
-        rs_in[sp] = rs_src[pl.ds(o * per, per)]
-        settle(rs_in, n - 1, all_recv.at[1])
-        zero = jnp.zeros((per, ALIGN, LANES), F32)
-        summed = lax.fori_loop(0, n, lambda i, t: t + rs_in[i].astype(F32), zero)
-        ag[o] = summed.astype(BF16)
+        rs_in[2 * sp + 1] = rs_src[pl.ds(o * per, per)]
+        settle(rs_in, 2 * n - 1, all_recv.at[1])
+        zero = jnp.zeros((2, per, ALIGN, LANES), F32)
+        summed = lax.fori_loop(
+            0, n, lambda i, t: t + rs_in[pl.ds(2 * i, 2)].astype(F32), zero, unroll=4
+        )
+        ag_src[...] = summed.astype(BF16)
+        ag[o] = ag_src[1]
 
         def send_ag(i, carry):
-            to = jnp.where(low_side, n - 1 - i, i)
-
-            @pl.when(to != sp)
-            def _():
-                remote(ag.at[o], ag.at[o], all_send.at[2], all_recv.at[2], (to, tp)).start()
+            for t in range(2):
+                @pl.when((i != sp) | (t != 1))
+                def _():
+                    remote(ag_src.at[t], ag.at[o],
+                           all_send.at[2], all_recv.at[2], (i, t)).start()
 
             return carry
 
         lax.fori_loop(0, n, send_ag, 0)
-
 
     def out_step(b):
         start = b * block
@@ -591,11 +599,7 @@
 
     @pl.when(is_owner)
     def _():
-        def sent(i, carry):
-            pltpu.make_async_copy(ag.at[0], ag.at[0], all_send.at[2]).wait()
-            return carry
-
-        lax.fori_loop(0, n - 1, sent, 0)
+        settle(rs_in, 2 * n - 1, all_send.at[2])
 
 
 def store(*refs):
@@ -670,14 +674,15 @@
             pltpu.VMEM((8, channels), F32),
             pltpu.VMEM((n, 2 * groups, LANES), BF16),
             pltpu.VMEM((owners.count * per, ALIGN, LANES), BF16),
-            pltpu.VMEM((n, per, ALIGN, LANES), BF16),
+            pltpu.VMEM((2 * n, per, ALIGN, LANES), BF16),
+            pltpu.VMEM((2, per, ALIGN, LANES), BF16),
             pltpu.VMEM((owners.count, per, ALIGN, LANES), BF16),
             pltpu.VMEM(plan.own.shape, BF16),
             pltpu.VMEM(plan.taps.shape, BF16),
             pltpu.VMEM((1, channels), F32),
             pltpu.VMEM((1, channels), F32),
             pltpu.SemaphoreType.REGULAR((3,)),
-            dma((9,)), dma((chunks,)), dma((4,)), dma((4,)),
+            dma((13,)), dma((chunks,)), dma((4,)), dma((4,)),
             dma((4,)), dma((4,)), dma((3,)), dma((3,)),
         ],
         compiler_params=pltpu.CompilerParams(

time: 24.2 us -> 22.9 us (0.946)
  Pallas kernels: 23.4 us -> 22.1 us
    pallas_call x1, Pallas kernels: 22.4 us -> 21.1 us  [shards(): pl.pallas_call(functools.partial(body, plan, n, tiles, owners, total), ou...]
where the time goes in v4:
time: 22.9 us; the launch traced here: 22.8 us
  Pallas kernels  22.1 us (97%)
  between operations  0.64 us (3%)
    pallas_call x1, Pallas kernels, shards(): pl.pallas_call(functools.partial(body, plan, n, tiles, owners, total), ou...  21.1 us
    pallas_call x1, Pallas kernels, shards(): pl.pallas_call(store, out_shape=(jax.ShapeDtypeStruct((rows, channels), B...  1.05 us

profile of v4, /device:TPU:0, one launch (start us, length us, event | category | flops | bytes accessed | tf_op | source)
XLA Modules:
  0.0 22.8 jit_solution(5784397768994286608)
XLA Ops:
  0.6 21.1 %shard_map.137 = (bf16[256,1024]{1,0:T(8,128)(2,1)S(1)}, bf16[256,1024]{1,0:T(8,128)(2,1)S(1)}, f32[31,1024]{1,0:T(8,128)S(1)}, f32[16,128]{1,0:T(8,128)S(1)}) custom-call(bf16[256,1024]{1,0:T(8,128)(2,1)} %value_h.1, bf16[256,1024]{1,0:T(8,128)(2,1)} %gate_h.1, f32[31,1024]{1,0:T(8,128)} %taps_h.1, f32[1,1024]{1,0:T(1,128)} %bitcast.4, f32[1,1024]{1,0:T(1,128)} %bitcast.5, ...), custom_call_target="tpu_custom_call" | custom-call | tf_op jit(solution)/shard_map/pallas_call | solution.py:638
  21.7 1.1 %shard_map.138 = (bf16[256,1024]{1,0:T(8,128)(2,1)}, bf16[256,1024]{1,0:T(8,128)(2,1)}, f32[31,1024]{1,0:T(8,128)}, f32[8,128]{1,0:T(8,128)}, f32[8,128]{1,0:T(8,128)}) custom-call(bf16[256,1024]{1,0:T(8,128)(2,1)S(1)} %get-tuple-element.14.refs_0_, bf16[256,1024]{1,0:T(8,128)(2,1)S(1)} %get-tuple-element.15.refs_1_, ...), custom_call_target="tpu_custom_call" | custom-call | tf_op jit(solution)/shard_map/pallas_call | solution.py:701

commit v5 on v4

--- a/solution.py
+++ b/solution.py
@@ -20,49 +20,63 @@
 
 class Plan:
     def __init__(self, rows, kernel, total):
-        self.half = kernel // 2
+        self.half = half = kernel // 2
         self.kernel = kernel
         self.rows = rows
-        self.edge = -(-self.half // ALIGN) * ALIGN
-        edge = self.edge
-        self.block = rows // 2
-        self.size = self.block + 2 * edge
-        size = self.size
-        self.freqs = size // 2
+        self.edge = edge = -(-half // ALIGN) * ALIGN
+        self.side = side = 4 * edge
+        self.inner = rows - 2 * edge
         self.wide = rows + 2 * edge
-        omega = 2.0 * np.pi * (np.arange(self.freqs) + 0.5) / size
-
-        def spectrum(times):
-            angle = omega[:, None] * times[None, :]
+        self.tap_rows = -(-kernel // ALIGN) * ALIGN
+
+        def omega(size):
+            return 2.0 * np.pi * (np.arange(size // 2) + 0.5) / size
+
+        def spectrum(size, times):
+            angle = omega(size)[:, None] * times[None, :]
             return np.concatenate([np.cos(angle), np.sin(angle)], 0)
 
-        def inverse(times):
-            angle = times[:, None] * omega[None, :]
+        def inverse(size, times):
+            angle = times[:, None] * omega(size)[None, :]
             return np.concatenate([np.cos(angle), -np.sin(angle)], 1)
 
-        own = np.arange(self.block)
-        self.tap_rows = -(-kernel // ALIGN) * ALIGN
-        lags = inverse(np.arange(self.tap_rows) - self.half)
-        lags[kernel:] = 0.0
-        self.mats = np.concatenate(
+        def lags(size):
+            out = inverse(size, np.arange(self.tap_rows) - half)
+            out[kernel:] = 0.0
+            return out
+
+        main = np.arange(self.inner) + edge
+        top = np.arange(edge) + edge
+        low = np.arange(edge) + side - 2 * edge
+        self.main = np.concatenate(
             [
-                spectrum(np.arange(size)),
-                inverse(own + edge - self.half),
-                inverse(own + edge + self.half),
-                lags,
+                spectrum(rows, np.arange(rows)), inverse(rows, main - half),
+                inverse(rows, main + half), lags(rows),
             ],
             0,
         )
-        self.at_conv = size
-        self.at_grad = self.at_conv + self.block
-        self.at_lags = self.at_grad + self.block
-        self.own = spectrum(own + edge)
-        taps = np.zeros((size, self.tap_rows))
-        taps[:, :kernel] = spectrum(np.arange(kernel)) * (2.0 / size)
+        self.at_conv = rows
+        self.at_grad = self.at_conv + self.inner
+        self.at_lags = self.at_grad + self.inner
+        self.edges = np.concatenate(
+            [spectrum(side, np.arange(side))]
+            + [inverse(side, part + shift) for shift in (-half, half) for part in (top, low)]
+            + [lags(side)],
+            0,
+        )
+        self.edge_conv = side
+        self.edge_grad = side + 2 * edge
+        self.edge_lags = side + 4 * edge
+        self.own = spectrum(rows, main)
+        self.own_edges = np.concatenate([spectrum(side, top), spectrum(side, low)], 0)
+        taps = np.zeros((rows + side, self.tap_rows))
+        times = np.arange(kernel)
+        taps[:rows, :kernel] = spectrum(rows, times) * (2.0 / rows)
+        taps[rows:, :kernel] = spectrum(side, times) * (2.0 / side)
         high = taps.astype(jnp.bfloat16)
-        low = taps - high.astype(np.float64)
-        self.taps = np.concatenate([high.astype(np.float64), high.astype(np.float64), low], 1)
-        self.lag_scale = 2.0 / size / math.sqrt(total)
+        low_part = taps - high.astype(np.float64)
+        self.taps = np.concatenate([high.astype(np.float64), high.astype(np.float64), low_part], 1)
+        self.lag_scale = [2.0 / size / math.sqrt(total) for size in (rows, side)]
 
 
 class Owners:
@@ -82,22 +96,21 @@
 
 def body(
     plan, n, tiles, owners, total,
-    value_h, gate_h, taps_h, gain_h, shift_h, w_h, go_h, mats_h, own_h, ft_h,
+    value_h, gate_h, taps_h, gain_h, shift_h, w_h, go_h, mats_h, emats_h, own_h, eown_h, ft_h,
     dv, dg, dt_o, dgs_o,
-    value, gate, taps, w, go, mats,
-    sig_s, gw, conv, gm, gcw, tcat, ts, g_spec, spec_s, dsp, prod,
+    value, gate, taps, w, go, mats, emats, own, eown,
+    sig_s, gw, conv, gm, gcw, tcat, ts, g_spec, spec_s, prod, lag_s,
     st1, st1_in, st2, st2_in, inv_s, colg, cols, hgain, hshift,
-    gs, rs_src, rs_in, ag_src, ag, own, ft, gain, shift,
+    gs, rs_src, rs_in, ag_src, ag, ft, gain, shift,
     meet, load_sem, w_sem, halo_send, halo_recv, tp_send, tp_recv,
     all_send, all_recv,
 ):
     sp = lax.axis_index("sp")
     tp = lax.axis_index("tp")
-    rows, edge, block = plan.rows, plan.edge, plan.block
+    rows, edge, side, inner_rows = plan.rows, plan.edge, plan.side, plan.inner
     channels = value.shape[1]
     width = channels * 2
     chunks = channels // CHUNK
-    size, freqs = plan.size, plan.freqs
     per = owners.per
     nxt = lax.rem(sp + 1, n)
     prv = lax.rem(sp + n - 1, n)
@@ -119,8 +132,10 @@
     sides = [pl.ds(0, edge), pl.ds(rows - edge, edge)]
     pairs = [(h.at[part], v.at[part]) for h, v in ((value_h, value), (gate_h, gate)) for part in sides]
     pairs += [(h.at[inner], v.at[inner]) for h, v in ((value_h, value), (gate_h, gate))]
-    pairs += [(taps_h, taps), (ft_h, ft), (go_h, go)]
-    late = [(mats_h, mats), (own_h, own), (gain_h, gain), (shift_h, shift)]
+    pairs += [(taps_h, taps), (ft_h, ft), (mats_h, mats), (go_h, go)]
+    late = [
+        (emats_h, emats), (own_h, own), (eown_h, eown), (gain_h, gain), (shift_h, shift),
+    ]
     loads = [
         pltpu.make_async_copy(a, b, load_sem.at[i]) for i, (a, b) in enumerate(pairs + late)
     ]
@@ -128,6 +143,48 @@
     def w_copy(c):
         part = pl.ds(pl.multiple_of(c * CHUNK, CHUNK), CHUNK)
         return pltpu.make_async_copy(w_h.at[part], w.at[part], w_sem.at[c])
+
+    def tell(sem, s, t):
+        pl.semaphore_signal(sem, 1, device_id=(s, t), device_id_type=pl.DeviceIdType.MESH)
+
+    members = 2 * jnp.minimum(crew, n - head)
+
+    def each_member(sem):
+        def step(i, carry):
+            s, t = head + i // 2, lax.rem(i, 2)
+
+            @pl.when((s != sp) | (t != tp))
+            def _():
+                tell(sem, s, t)
+
+            return carry
+
+        lax.fori_loop(0, members, step, 0)
+
+    def each_head(sem):
+        def step(i, carry):
+            @pl.when(i * crew != sp)
+            def _():
+                tell(sem, i * crew, 1)
+
+            return carry
+
+        lax.fori_loop(0, crews, step, 0)
+
+    tell(barrier, sp, 1 - tp)
+
+    @pl.when(has_prv)
+    def _():
+        tell(barrier, prv, tp)
+
+    @pl.when(has_nxt)
+    def _():
+        tell(barrier, nxt, tp)
+
+    @pl.when(is_head)
+    def _():
+        each_member(barrier)
+        each_head(barrier)
 
     for load in loads[: len(pairs)]:
         load.start()
@@ -135,48 +192,6 @@
         w_copy(c).start()
     for load in loads[len(pairs):]:
         load.start()
-
-    def tell(sem, s, t):
-        pl.semaphore_signal(sem, 1, device_id=(s, t), device_id_type=pl.DeviceIdType.MESH)
-
-    members = 2 * jnp.minimum(crew, n - head)
-
-    def each_member(sem):
-        def step(i, carry):
-            s, t = head + i // 2, lax.rem(i, 2)
-
-            @pl.when((s != sp) | (t != tp))
-            def _():
-                tell(sem, s, t)
-
-            return carry
-
-        lax.fori_loop(0, members, step, 0)
-
-    def each_head(sem):
-        def step(i, carry):
-            @pl.when(i * crew != sp)
-            def _():
-                tell(sem, i * crew, 1)
-
-            return carry
-
-        lax.fori_loop(0, crews, step, 0)
-
-    tell(barrier, sp, 1 - tp)
-
-    @pl.when(has_prv)
-    def _():
-        tell(barrier, prv, tp)
-
-    @pl.when(has_nxt)
-    def _():
-        tell(barrier, nxt, tp)
-
-    @pl.when(is_head)
-    def _():
-        each_member(barrier)
-        each_head(barrier)
 
     greeted = (
         1 + has_prv.astype(jnp.int32) + has_nxt.astype(jnp.int32)
@@ -314,11 +329,6 @@
         gm[:, part] = mix(go[...], w[part])
         return carry
 
-    loads[8].wait()
-    lax.fori_loop(0, chunks, mix_step, 0)
-    handshake_across()
-    loads[9].wait()
-
     def fold(x):
         out = x[:, :LANES]
         for k in range(1, x.shape[1] // LANES):
@@ -327,57 +337,88 @@
 
     lanes = lax.broadcasted_iota(jnp.int32, (ALIGN, LANES), 1) < LANES // 2
 
-    def multiply(spec, sign):
+    def multiply(at, size, tap_at, sign, source):
+        freqs = size // 2
         for f in range(0, freqs, ALIGN):
-            high, low = pl.ds(f, ALIGN), pl.ds(freqs + f, ALIGN)
+            high, low = pl.ds(at + f, ALIGN), pl.ds(at + freqs + f, ALIGN)
             for c in range(chunks):
-                re, im = spec[high, cut(c)], spec[low, cut(c)]
-                ta, tb = ts[high, cut(c)], ts[low, cut(c)]
+                re, im = source[high, cut(c)], source[low, cut(c)]
+                ta = ts[pl.ds(tap_at + f, ALIGN), cut(c)]
+                tb = ts[pl.ds(tap_at + freqs + f, ALIGN), cut(c)]
                 prod[high, cut(c)] = (re * ta + sign * im * tb).astype(BF16)
                 other = re * tb - sign * im * ta
                 prod[low, cut(c)] = (sign * other).astype(BF16)
 
-    def conv_step(b):
-        start = b * block
-        spec = g_spec.at[pl.ds(b * size, size)]
-        spec[...] = dot(mats[pl.ds(0, size)], gw[pl.ds(start, size)])
-        multiply(spec, 1.0)
-        conv[pl.ds(start, block)] = dot(mats[pl.ds(plan.at_conv, block)], prod[...])
-        for r in range(start, start + block, ALIGN):
+    def slot(r):
+        return r - edge if edge <= r < rows - edge else (r + inner_rows if r < edge else r)
+
+    main_rows = list(range(edge, rows - edge, ALIGN))
+    middle = len(main_rows) // 2
+    first_rows, second_rows = main_rows[:middle], main_rows[middle:]
+    edge_rows = list(range(0, edge, ALIGN)) + list(range(rows - edge, rows, ALIGN))
+
+    def stats(picked):
+        for r in picked:
             one = two = None
             for c in range(chunks):
                 x = conv[pl.ds(r, ALIGN), cut(c)]
                 p, q = fold(x), fold(x * x)
                 one, two = (p, q) if c == 0 else (one + p, two + q)
-            st1[pl.ds(r, ALIGN)] = jnp.where(
+            st1[pl.ds(slot(r), ALIGN)] = jnp.where(
                 lanes, jnp.sum(one, 1, keepdims=True), jnp.sum(two, 1, keepdims=True)
             )
 
-    def swap(src, dst, b, k):
-        place = pl.ds(b * block, block)
+    def transform_main(source, target, at, sign):
+        target[pl.ds(0, rows)] = dot(mats[pl.ds(0, rows)], source[pl.ds(edge, rows)])
+        multiply(0, rows, 0, sign, target)
+        conv[pl.ds(edge, inner_rows)] = dot(mats[pl.ds(at, inner_rows)], prod[pl.ds(0, rows)])
+
+    def transform_edge(e, source, target, at, sign):
+        place = rows + e * side
+        window = source[pl.ds(e * (plan.wide - side), side)]
+        target[pl.ds(place, side)] = dot(emats[pl.ds(0, side)], window)
+        multiply(place, side, rows, sign, target)
+        conv[pl.ds(e * (rows - edge), edge)] = dot(
+            emats[pl.ds(at + e * edge, edge)], prod[pl.ds(place, side)]
+        )
+
+    def swap(src, dst, start, count, k):
+        place = pl.ds(start, count)
         return remote(
             src.at[place], dst.at[place], tp_send.at[k], tp_recv.at[k], (sp, 1 - tp)
         )
 
-    swap1 = [swap(st1, st1_in, b, b) for b in range(2)]
-    swap2 = [swap(st2, st2_in, b, 2 + b) for b in range(2)]
-
-    def conv_at(b):
-        def step(_, carry):
-            conv_step(b)
-            return carry
-
-        lax.fori_loop(0, 1, step, 0)
-
+    cutoff = middle * ALIGN
+    swap1 = [
+        swap(st1, st1_in, 0, inner_rows, 0), swap(st1, st1_in, inner_rows, 2 * edge, 1)
+    ]
+    swap2 = [
+        swap(st2, st2_in, 0, cutoff, 2), swap(st2, st2_in, cutoff, inner_rows - cutoff, 3),
+        swap(st2, st2_in, inner_rows, 2 * edge, 4),
+    ]
+
+    def conv_main_phase():
+        transform_main(gw, g_spec, plan.at_conv, 1.0)
+        stats(main_rows)
+
+    def conv_edge_phase():
+        transform_edge(0, gw, g_spec, plan.edge_conv, 1.0)
+        transform_edge(1, gw, g_spec, plan.edge_conv, 1.0)
+        stats(edge_rows)
+
+    loads[8].wait()
+    conv_main_phase()
+    swap1[0].start()
+    loads[9].wait()
+    lax.fori_loop(0, chunks, mix_step, 0)
+    handshake_across()
+    for load in loads[10:]:
+        load.wait()
     recv_prv(gw_halo, gw)
-    conv_at(0)
-    swap1[0].start()
     recv_nxt(gw_halo, gw)
-    conv_at(1)
+    conv_edge_phase()
     swap1[1].start()
     handshake_down()
-    for load in loads[10:]:
-        load.wait()
     hgain[...] = jnp.broadcast_to(0.5 * gain[...], hgain.shape)
     hshift[...] = jnp.broadcast_to(0.5 * shift[...], hshift.shape)
 
@@ -387,15 +428,15 @@
     def halves(x):
         return x[:8] + x[8:]
 
-    def norm_at(b):
+    def norm_at(picked, opening):
         total_g, total_s = [None] * chunks, [None] * chunks
-        for r in range(b * block, (b + 1) * block, ALIGN):
-            part = pl.ds(r, ALIGN)
-            tot = (st1[part] + st1_in[part]) * (1.0 / width)
+        for r in picked:
+            part, place = pl.ds(r, ALIGN), pl.ds(slot(r), ALIGN)
+            tot = (st1[place] + st1_in[place]) * (1.0 / width)
             mean = tot[:, :1]
             var = tot[:, LANES // 2 : LANES // 2 + 1] - mean * mean
             inv = lax.rsqrt(var + EPS)
-            inv_s[part] = jnp.broadcast_to(inv, (ALIGN, LANES))
+            inv_s[place] = jnp.broadcast_to(inv, (ALIGN, LANES))
             one = two = None
             for c in range(chunks):
                 hg = twice(hgain[:, cut(c)])
@@ -413,11 +454,11 @@
                 if total_g[c] is not None:
                     g, h = total_g[c] + g, total_s[c] + h
                 total_g[c], total_s[c] = g, h
-            st2[part] = jnp.where(
+            st2[place] = jnp.where(
                 lanes, jnp.sum(one, 1, keepdims=True), jnp.sum(two, 1, keepdims=True)
             )
         for c in range(chunks):
-            if b == 0:
+            if opening:
                 colg[:, cut(c)] = total_g[c]
                 cols[:, cut(c)] = total_s[c]
             else:
@@ -425,11 +466,13 @@
                 cols[:, cut(c)] += total_s[c]
 
     swap1[0].wait_recv()
-    norm_at(0)
+    norm_at(first_rows, True)
     swap2[0].start()
+    norm_at(second_rows, False)
+    swap2[1].start()
     swap1[1].wait_recv()
-    norm_at(1)
-    swap2[1].start()
+    norm_at(edge_rows, False)
+    swap2[2].start()
 
     rg = jnp.sum(colg[...], 0, keepdims=True)
     rsh = jnp.sum(cols[...], 0, keepdims=True)
@@ -445,11 +488,11 @@
     handshake_done()
     lax.fori_loop(1, n, send_gs, 0)
 
-    def gc_at(b):
-        for r in range(b * block, (b + 1) * block, ALIGN):
-            part = pl.ds(r, ALIGN)
-            tot = (st2[part] + st2_in[part]) * (1.0 / width)
-            inv = inv_s[part]
+    def gc_at(picked):
+        for r in picked:
+            part, place = pl.ds(r, ALIGN), pl.ds(slot(r), ALIGN)
+            tot = (st2[place] + st2_in[place]) * (1.0 / width)
+            inv = inv_s[place]
             scaled = inv * tot
             m1 = scaled[:, :1]
             m2 = scaled[:, LANES // 2 : LANES // 2 + 1]
@@ -464,12 +507,11 @@
         rs_src[pl.ds(tiles, slots - tiles)] = jnp.zeros((slots - tiles, ALIGN, LANES), BF16)
     tall = plan.tap_rows // ALIGN
 
-    def lag_part(b, f, c):
-        high, low = pl.ds(f, ALIGN), pl.ds(freqs + f, ALIGN)
+    def lag_part(at, size, f, c):
+        high, low = pl.ds(at + f, ALIGN), pl.ds(at + size // 2 + f, ALIGN)
         re, im = spec_s[high, cut(c)], spec_s[low, cut(c)]
-        hr = g_spec[pl.ds(b * size + f, ALIGN), cut(c)]
-        hi = g_spec[pl.ds(b * size + freqs + f, ALIGN), cut(c)]
-        return high, low, hr * re + hi * im, hr * im - hi * re
+        hr, hi = g_spec[high, cut(c)], g_spec[low, cut(c)]
+        return hr * re + hi * im, hr * im - hi * re
 
     def send_rs(i, carry):
         o = jnp.where(low_side, owners.count - 1 - i, i)
@@ -482,70 +524,81 @@
 
         return carry
 
-    def spec_first(_, carry):
-        spec_s[...] = dot(own[...], gcw[pl.ds(edge, block)])
-        for f in range(0, freqs, ALIGN):
+    def spec_main_phase():
+        spec_s[pl.ds(0, rows)] = dot(own[...], gcw[pl.ds(2 * edge, inner_rows)])
+        for f in range(0, rows // 2, ALIGN):
             for c in range(chunks):
-                high, low, dr, di = lag_part(0, f, c)
-                dsp[high, cut(c)] = dr
-                dsp[low, cut(c)] = di
-        return carry
-
-    def spec_last(_, carry):
-        spec_s[...] = dot(own[...], gcw[pl.ds(edge + block, block)])
-        for f in range(0, freqs, ALIGN):
+                dr, di = lag_part(0, rows, f, c)
+                prod[pl.ds(f, ALIGN), cut(c)] = dr.astype(BF16)
+                prod[pl.ds(rows // 2 + f, ALIGN), cut(c)] = di.astype(BF16)
+        lag_s[...] = (
+            dot(mats[pl.ds(plan.at_lags, plan.tap_rows)], prod[pl.ds(0, rows)])
+            * plan.lag_scale[0]
+        )
+
+    def spec_edge_phase():
+        for e in range(2):
+            spec_s[pl.ds(rows + e * side, side)] = dot(
+                eown[pl.ds(e * side, side)], gcw[pl.ds(edge + e * (rows - edge), edge)]
+            )
+        for f in range(0, side // 2, ALIGN):
             for c in range(chunks):
-                high, low, dr, di = lag_part(1, f, c)
-                prod[high, cut(c)] = (dr + dsp[high, cut(c)]).astype(BF16)
-                prod[low, cut(c)] = (di + dsp[low, cut(c)]).astype(BF16)
-        out = dot(mats[pl.ds(plan.at_lags, plan.tap_rows)], prod[...]) * plan.lag_scale
+                r0, i0 = lag_part(rows, side, f, c)
+                r1, i1 = lag_part(rows + side, side, f, c)
+                prod[pl.ds(rows + f, ALIGN), cut(c)] = (r0 + r1).astype(BF16)
+                prod[pl.ds(rows + side // 2 + f, ALIGN), cut(c)] = (i0 + i1).astype(BF16)
+        out = lag_s[...] + plan.lag_scale[1] * dot(
+            emats[pl.ds(plan.edge_lags, plan.tap_rows)], prod[pl.ds(rows, side)]
+        )
         out = out.astype(BF16)
         for r in range(tall):
             for k in range(groups):
                 rs_src[k * tall + r] = out[
                     r * ALIGN : (r + 1) * ALIGN, k * LANES : (k + 1) * LANES
                 ]
-        return carry
 
     swap2[0].wait_recv()
-    gc_at(0)
-    lax.fori_loop(0, 1, spec_first, 0)
+    gc_at(first_rows)
     swap2[1].wait_recv()
-    gc_at(1)
-
-    lax.fori_loop(0, 1, spec_last, 0)
+    gc_at(second_rows)
+    spec_main_phase()
+    swap2[2].wait_recv()
+    gc_at(edge_rows)
+    spec_edge_phase()
     lax.fori_loop(0, owners.count, send_rs, 0)
     send_halo(gc_halo)
 
-    @pl.when(is_owner)
-    def _():
-        o = sp - owners.first
-        rs_in[2 * sp + 1] = rs_src[pl.ds(o * per, per)]
-        settle(rs_in, 2 * n - 1, all_recv.at[1])
-        zero = jnp.zeros((2, per, ALIGN, LANES), F32)
-        summed = lax.fori_loop(
-            0, n, lambda i, t: t + rs_in[pl.ds(2 * i, 2)].astype(F32), zero, unroll=4
-        )
-        ag_src[...] = summed.astype(BF16)
-        ag[o] = ag_src[1]
-
-        def send_ag(i, carry):
-            for t in range(2):
-                @pl.when((i != sp) | (t != 1))
-                def _():
-                    remote(ag_src.at[t], ag.at[o],
-                           all_send.at[2], all_recv.at[2], (i, t)).start()
-
-            return carry
-
-        lax.fori_loop(0, n, send_ag, 0)
-
-    def out_step(b):
-        start = b * block
-        spec_s[...] = dot(mats[pl.ds(0, size)], gcw[pl.ds(start, size)])
-        multiply(spec_s, -1.0)
-        conv[pl.ds(start, block)] = dot(mats[pl.ds(plan.at_grad, block)], prod[...])
-        for r in range(start, start + block, ALIGN):
+    def sum_phase():
+        @pl.when(is_owner)
+        def _():
+            o = sp - owners.first
+            rs_in[2 * sp + 1] = rs_src[pl.ds(o * per, per)]
+            settle(rs_in, 2 * n - 1, all_recv.at[1])
+            zero = jnp.zeros((2, per, ALIGN, LANES), F32)
+            summed = lax.fori_loop(
+                0, n, lambda i, t: t + rs_in[pl.ds(2 * i, 2)].astype(F32), zero, unroll=4
+            )
+            ag_src[...] = summed.astype(BF16)
+            ag[o] = ag_src[1]
+
+    def gather_phase(first, count):
+        @pl.when(is_owner)
+        def _():
+            o = sp - owners.first
+
+            def send_ag(i, carry):
+                for t in range(2):
+                    @pl.when((i != sp) | (t != 1))
+                    def _():
+                        remote(ag_src.at[t], ag.at[o],
+                               all_send.at[2], all_recv.at[2], (i, t)).start()
+
+                return carry
+
+            lax.fori_loop(first, first + count, send_ag, 0)
+
+    def finish(picked):
+        for r in picked:
             part = pl.ds(r, ALIGN)
             for c in range(chunks):
                 sig = sig_s[part, cut(c)]
@@ -555,18 +608,22 @@
                     left * value[part, cut(c)].astype(F32) * (1.0 - sig)
                 ).astype(BF16)
 
-    def out_at(b):
-        def step(_, carry):
-            out_step(b)
-            return carry
-
-        lax.fori_loop(0, 1, step, 0)
-
+    def out_main_phase():
+        transform_main(gcw, spec_s, plan.at_grad, -1.0)
+        finish(main_rows)
+
+    def out_edge_phase():
+        transform_edge(0, gcw, spec_s, plan.edge_grad, -1.0)
+        transform_edge(1, gcw, spec_s, plan.edge_grad, -1.0)
+        finish(edge_rows)
+
+    out_main_phase()
+    sum_phase()
+    gather_phase(0, 1)
+    gather_phase(1, n - 1)
     recv_prv(gc_halo, gcw)
-    out_at(0)
     recv_nxt(gc_halo, gcw)
-    out_at(1)
-
+    out_edge_phase()
     settle(gs, n - 1, all_recv.at[0])
     small = lax.fori_loop(
         0, n, lambda i, t: t + gs[i].astype(F32), jnp.zeros(gs.shape[1:], F32)
@@ -575,9 +632,8 @@
 
     sent_halo(gw_halo)
     sent_halo(gc_halo)
-    for k in range(2):
-        swap1[k].wait_send()
-        swap2[k].wait_send()
+    for each in swap1 + swap2:
+        each.wait_send()
     settle(gs, n - 1, all_send.at[0])
 
     @pl.when(is_owner)
@@ -627,12 +683,14 @@
     owners = Owners(n, tiles)
     per = owners.per
     model = grad_out.shape[1]
-    mats = jnp.asarray(plan.mats, BF16)
+    mats = jnp.asarray(plan.main, BF16)
+    emats = jnp.asarray(plan.edges, BF16)
     own = jnp.asarray(plan.own, BF16)
+    eown = jnp.asarray(plan.own_edges, BF16)
     ft = jnp.asarray(plan.taps, BF16)
     hbm = pl.BlockSpec(memory_space=pltpu.HBM)
     vmem = pl.BlockSpec(memory_space=pltpu.VMEM)
-    size, block = plan.size, plan.block
+    both = rows + 2 * plan.side
     chunks = channels // CHUNK
     dma = pltpu.SemaphoreType.DMA
     results = pl.pallas_call(
@@ -643,7 +701,7 @@
             pltpu.VMEM((kernel, channels), F32),
             pltpu.VMEM((2 * groups, LANES), F32),
         ),
-        in_specs=[hbm] * 10,
+        in_specs=[hbm] * 12,
         out_specs=(vmem,) * 4,
         scratch_shapes=[
             pltpu.VMEM((rows, channels), BF16),
@@ -651,18 +709,21 @@
             pltpu.VMEM((kernel, channels), F32),
             pltpu.VMEM((channels, model), BF16),
             pltpu.VMEM((rows, model), BF16),
-            pltpu.VMEM(plan.mats.shape, BF16),
+            pltpu.VMEM(plan.main.shape, BF16),
+            pltpu.VMEM(plan.edges.shape, BF16),
+            pltpu.VMEM(plan.own.shape, BF16),
+            pltpu.VMEM(plan.own_edges.shape, BF16),
             pltpu.VMEM((rows, channels), F32),
             pltpu.VMEM((plan.wide, channels), BF16),
             pltpu.VMEM((rows, channels), F32),
             pltpu.VMEM((rows, channels), F32),
             pltpu.VMEM((plan.wide, channels), BF16),
             pltpu.VMEM((3 * plan.tap_rows, channels), BF16),
-            pltpu.VMEM((size, channels), F32),
-            pltpu.VMEM((2 * size, channels), F32),
-            pltpu.VMEM((size, channels), F32),
-            pltpu.VMEM((size, channels), F32),
-            pltpu.VMEM((size, channels), BF16),
+            pltpu.VMEM((rows + plan.side, channels), F32),
+            pltpu.VMEM((both, channels), F32),
+            pltpu.VMEM((both, channels), F32),
+            pltpu.VMEM((both, channels), BF16),
+            pltpu.VMEM((plan.tap_rows, channels), F32),
             pltpu.VMEM((rows, LANES), F32),
             pltpu.VMEM((rows, LANES), F32),
             pltpu.VMEM((rows, LANES), F32),
@@ -677,13 +738,12 @@
             pltpu.VMEM((2 * n, per, ALIGN, LANES), BF16),
             pltpu.VMEM((2, per, ALIGN, LANES), BF16),
             pltpu.VMEM((owners.count, per, ALIGN, LANES), BF16),
-            pltpu.VMEM(plan.own.shape, BF16),
             pltpu.VMEM(plan.taps.shape, BF16),
             pltpu.VMEM((1, channels), F32),
             pltpu.VMEM((1, channels), F32),
             pltpu.SemaphoreType.REGULAR((3,)),
-            dma((13,)), dma((chunks,)), dma((4,)), dma((4,)),
-            dma((4,)), dma((4,)), dma((3,)), dma((3,)),
+            dma((15,)), dma((chunks,)), dma((4,)), dma((4,)),
+            dma((5,)), dma((5,)), dma((3,)), dma((3,)),
         ],
         compiler_params=pltpu.CompilerParams(
             collective_id=0, has_side_effects=True, vmem_limit_bytes=VMEM_GRANT
@@ -693,7 +753,7 @@
             pltpu.with_memory_space_constraint(x, pltpu.HBM)
             for x in (
                 value_in, gate_in, taps, gain.reshape(1, -1), shift.reshape(1, -1), w_out,
-                grad_out, mats, own, ft,
+                grad_out, mats, emats, own, eown, ft,
             )
         )
     )

time: 22.9 us -> 22.7 us (level)
  no operation moved by 1% of the time
where the time goes in v5:
time: 22.7 us; the launch traced here: 22.6 us
  Pallas kernels  22 us (97%)
  between operations  0.64 us (3%)
    pallas_call x1, Pallas kernels, shards(): pl.pallas_call(functools.partial(body, plan, n, tiles, owners, total), ou...  20.9 us
    pallas_call x1, Pallas kernels, shards(): pl.pallas_call(store, out_shape=(jax.ShapeDtypeStruct((rows, channels), B...  1.05 us

profile of v5, /device:TPU:0, one launch (start us, length us, event | category | flops | bytes accessed | tf_op | source)
XLA Modules:
  0.0 22.6 jit_solution(6396230119783867855)
XLA Ops:
  0.6 20.9 %shard_map.155 = (bf16[256,1024]{1,0:T(8,128)(2,1)S(1)}, bf16[256,1024]{1,0:T(8,128)(2,1)S(1)}, f32[31,1024]{1,0:T(8,128)S(1)}, f32[16,128]{1,0:T(8,128)S(1)}) custom-call(bf16[256,1024]{1,0:T(8,128)(2,1)} %value_h.1, bf16[256,1024]{1,0:T(8,128)(2,1)} %gate_h.1, f32[31,1024]{1,0:T(8,128)} %taps_h.1, f32[1,1024]{1,0:T(1,128)} %bitcast.4, f32[1,1024]{1,0:T(1,128)} %bitcast.5, ...), custom_call_target="tpu_custom_call" | custom-call | tf_op jit(solution)/shard_map/pallas_call | solution.py:696
  21.5 1.1 %shard_map.156 = (bf16[256,1024]{1,0:T(8,128)(2,1)}, bf16[256,1024]{1,0:T(8,128)(2,1)}, f32[31,1024]{1,0:T(8,128)}, f32[8,128]{1,0:T(8,128)}, f32[8,128]{1,0:T(8,128)}) custom-call(bf16[256,1024]{1,0:T(8,128)(2,1)S(1)} %get-tuple-element.14.refs_0_, bf16[256,1024]{1,0:T(8,128)(2,1)S(1)} %get-tuple-element.15.refs_1_, ...), custom_call_target="tpu_custom_call" | custom-call | tf_op jit(solution)/shard_map/pallas_call | solution.py:761

commit v6 on v5

--- a/solution.py
+++ b/solution.py
@@ -373,14 +373,16 @@
         multiply(0, rows, 0, sign, target)
         conv[pl.ds(edge, inner_rows)] = dot(mats[pl.ds(at, inner_rows)], prod[pl.ds(0, rows)])
 
-    def transform_edge(e, source, target, at, sign):
-        place = rows + e * side
-        window = source[pl.ds(e * (plan.wide - side), side)]
-        target[pl.ds(place, side)] = dot(emats[pl.ds(0, side)], window)
-        multiply(place, side, rows, sign, target)
-        conv[pl.ds(e * (rows - edge), edge)] = dot(
-            emats[pl.ds(at + e * edge, edge)], prod[pl.ds(place, side)]
-        )
+    def transform_edges(source, target, at, sign):
+        for e in range(2):
+            window = source[pl.ds(e * (plan.wide - side), side)]
+            target[pl.ds(rows + e * side, side)] = dot(emats[pl.ds(0, side)], window)
+        for e in range(2):
+            multiply(rows + e * side, side, rows, sign, target)
+        for e in range(2):
+            conv[pl.ds(e * (rows - edge), edge)] = dot(
+                emats[pl.ds(at + e * edge, edge)], prod[pl.ds(rows + e * side, side)]
+            )
 
     def swap(src, dst, start, count, k):
         place = pl.ds(start, count)
@@ -402,23 +404,17 @@
         stats(main_rows)
 
     def conv_edge_phase():
-        transform_edge(0, gw, g_spec, plan.edge_conv, 1.0)
-        transform_edge(1, gw, g_spec, plan.edge_conv, 1.0)
+        transform_edges(gw, g_spec, plan.edge_conv, 1.0)
         stats(edge_rows)
 
     loads[8].wait()
     conv_main_phase()
     swap1[0].start()
+    handshake_across()
     loads[9].wait()
     lax.fori_loop(0, chunks, mix_step, 0)
-    handshake_across()
     for load in loads[10:]:
         load.wait()
-    recv_prv(gw_halo, gw)
-    recv_nxt(gw_halo, gw)
-    conv_edge_phase()
-    swap1[1].start()
-    handshake_down()
     hgain[...] = jnp.broadcast_to(0.5 * gain[...], hgain.shape)
     hshift[...] = jnp.broadcast_to(0.5 * shift[...], hshift.shape)
 
@@ -465,29 +461,6 @@
                 colg[:, cut(c)] += total_g[c]
                 cols[:, cut(c)] += total_s[c]
 
-    swap1[0].wait_recv()
-    norm_at(first_rows, True)
-    swap2[0].start()
-    norm_at(second_rows, False)
-    swap2[1].start()
-    swap1[1].wait_recv()
-    norm_at(edge_rows, False)
-    swap2[2].start()
-
-    rg = jnp.sum(colg[...], 0, keepdims=True)
-    rsh = jnp.sum(cols[...], 0, keepdims=True)
-    groups = channels // LANES
-    gs[sp] = jnp.concatenate(
-        [x[:, k * LANES : (k + 1) * LANES] for x in (rg, rsh) for k in range(groups)], 0
-    ).astype(BF16)
-
-    def send_gs(d, carry):
-        remote(gs.at[sp], gs.at[sp], all_send.at[0], all_recv.at[0], (peer(d), tp)).start()
-        return carry
-
-    handshake_done()
-    lax.fori_loop(1, n, send_gs, 0)
-
     def gc_at(picked):
         for r in picked:
             part, place = pl.ds(r, ALIGN), pl.ds(slot(r), ALIGN)
@@ -501,6 +474,36 @@
                 gcw[pl.ds(r + edge, ALIGN), cut(c)] = (
                     inv * gm[part, cut(c)] - m1 - conv[part, cut(c)] * m2
                 ).astype(BF16)
+
+    swap1[0].wait_recv()
+    norm_at(first_rows, True)
+    swap2[0].start()
+    recv_prv(gw_halo, gw)
+    recv_nxt(gw_halo, gw)
+    conv_edge_phase()
+    swap1[1].start()
+    handshake_down()
+    norm_at(second_rows, False)
+    swap2[1].start()
+    swap2[0].wait_recv()
+    gc_at(first_rows)
+    swap1[1].wait_recv()
+    norm_at(edge_rows, False)
+    swap2[2].start()
+
+    rg = jnp.sum(colg[...], 0, keepdims=True)
+    rsh = jnp.sum(cols[...], 0, keepdims=True)
+    groups = channels // LANES
+    gs[sp] = jnp.concatenate(
+        [x[:, k * LANES : (k + 1) * LANES] for x in (rg, rsh) for k in range(groups)], 0
+    ).astype(BF16)
+
+    def send_gs(d, carry):
+        remote(gs.at[sp], gs.at[sp], all_send.at[0], all_recv.at[0], (peer(d), tp)).start()
+        return carry
+
+    handshake_done()
+    lax.fori_loop(1, n, send_gs, 0)
 
     slots = owners.count * per
     if slots > tiles:
@@ -557,8 +560,6 @@
                     r * ALIGN : (r + 1) * ALIGN, k * LANES : (k + 1) * LANES
                 ]
 
-    swap2[0].wait_recv()
-    gc_at(first_rows)
     swap2[1].wait_recv()
     gc_at(second_rows)
     spec_main_phase()
@@ -613,8 +614,7 @@
         finish(main_rows)
 
     def out_edge_phase():
-        transform_edge(0, gcw, spec_s, plan.edge_grad, -1.0)
-        transform_edge(1, gcw, spec_s, plan.edge_grad, -1.0)
+        transform_edges(gcw, spec_s, plan.edge_grad, -1.0)
         finish(edge_rows)
 
     out_main_phase()

time: 22.7 us -> 22.4 us (0.987)
  Pallas kernels: 22 us -> 21.6 us
    pallas_call x1, Pallas kernels: 20.9 us -> 20.6 us  [shards(): pl.pallas_call(functools.partial(body, plan, n, tiles, owners, total), ou...]
where the time goes in v6:
time: 22.4 us; the launch traced here: 22.3 us
  Pallas kernels  21.6 us (96%)
  between operations  0.64 us (3%)
    pallas_call x1, Pallas kernels, shards(): pl.pallas_call(functools.partial(body, plan, n, tiles, owners, total), ou...  20.6 us
    pallas_call x1, Pallas kernels, shards(): pl.pallas_call(store, out_shape=(jax.ShapeDtypeStruct((rows, channels), B...  1.05 us

profile of v6, /device:TPU:0, one launch (start us, length us, event | category | flops | bytes accessed | tf_op | source)
XLA Modules:
  0.0 22.3 jit_solution(1692394495278744380)
XLA Ops:
  0.6 20.6 %shard_map.155 = (bf16[256,1024]{1,0:T(8,128)(2,1)S(1)}, bf16[256,1024]{1,0:T(8,128)(2,1)S(1)}, f32[31,1024]{1,0:T(8,128)S(1)}, f32[16,128]{1,0:T(8,128)S(1)}) custom-call(bf16[256,1024]{1,0:T(8,128)(2,1)} %value_h.1, bf16[256,1024]{1,0:T(8,128)(2,1)} %gate_h.1, f32[31,1024]{1,0:T(8,128)} %taps_h.1, f32[1,1024]{1,0:T(1,128)} %bitcast.4, f32[1,1024]{1,0:T(1,128)} %bitcast.5, ...), custom_call_target="tpu_custom_call" | custom-call | tf_op jit(solution)/shard_map/pallas_call | solution.py:696
  21.2 1.1 %shard_map.156 = (bf16[256,1024]{1,0:T(8,128)(2,1)}, bf16[256,1024]{1,0:T(8,128)(2,1)}, f32[31,1024]{1,0:T(8,128)}, f32[8,128]{1,0:T(8,128)}, f32[8,128]{1,0:T(8,128)}) custom-call(bf16[256,1024]{1,0:T(8,128)(2,1)S(1)} %get-tuple-element.14.refs_0_, bf16[256,1024]{1,0:T(8,128)(2,1)S(1)} %get-tuple-element.15.refs_1_, ...), custom_call_target="tpu_custom_call" | custom-call | tf_op jit(solution)/shard_map/pallas_call | solution.py:761

commit v7 on v6

--- a/solution.py
+++ b/solution.py
@@ -83,7 +83,7 @@
     def __init__(self, n, tiles):
         self.count = max(1, min(n // 2, tiles))
         self.per = -(-tiles // self.count)
-        self.first = (n - self.count) // 2
+        self.first = max(0, (n - self.count) // 2 - 1)
 
 
 def dot(a, b):
@@ -131,8 +131,9 @@
     inner = pl.ds(edge, rows - 2 * edge)
     sides = [pl.ds(0, edge), pl.ds(rows - edge, edge)]
     pairs = [(h.at[part], v.at[part]) for h, v in ((value_h, value), (gate_h, gate)) for part in sides]
+    pairs += [(taps_h, taps), (ft_h, ft)]
     pairs += [(h.at[inner], v.at[inner]) for h, v in ((value_h, value), (gate_h, gate))]
-    pairs += [(taps_h, taps), (ft_h, ft), (mats_h, mats), (go_h, go)]
+    pairs += [(mats_h, mats), (go_h, go)]
     late = [
         (emats_h, emats), (own_h, own), (eown_h, eown), (gain_h, gain), (shift_h, shift),
     ]
@@ -187,10 +188,6 @@
         each_head(barrier)
 
     for load in loads[: len(pairs)]:
-        load.start()
-    for c in range(chunks):
-        w_copy(c).start()
-    for load in loads[len(pairs):]:
         load.start()
 
     greeted = (
@@ -292,6 +289,10 @@
 
     for load in loads[:4]:
         load.wait()
+    for c in range(chunks):
+        w_copy(c).start()
+    for load in loads[len(pairs):]:
+        load.start()
     sided = edge // ALIGN
     for r in range(sided):
         gate_step(r, 0)
@@ -301,9 +302,6 @@
     handshake_up()
     loads[4].wait()
     loads[5].wait()
-    lax.fori_loop(sided, rows // ALIGN - sided, gate_step, 0, unroll=7)
-    loads[6].wait()
-    loads[7].wait()
 
     tap = jnp.concatenate(
         [taps[...], jnp.zeros((plan.tap_rows - plan.kernel, channels), F32)], 0
@@ -313,12 +311,14 @@
     for k, part in enumerate((tap_high, tap_low, tap_high)):
         tcat[pl.ds(k * plan.tap_rows, plan.tap_rows)] = part
 
-    def tap_step(_, carry):
+    def tap_phase():
         for c in range(chunks):
             ts[:, cut(c)] = dot(ft[...], tcat[:, cut(c)])
-        return carry
-
-    lax.fori_loop(0, 1, tap_step, 0)
+
+    tap_phase()
+    loads[6].wait()
+    loads[7].wait()
+    lax.fori_loop(sided, rows // ALIGN - sided, gate_step, 0, unroll=7)
 
     def mix(a, b):
         return lax.dot_general(a, b, (((1,), (1,)), ((), ())), preferred_element_type=F32)

time: 22.4 us -> 22 us (0.982)
  Pallas kernels: 21.6 us -> 21.2 us
    pallas_call x1, Pallas kernels: 20.6 us -> 20.2 us  [shards(): pl.pallas_call(functools.partial(body, plan, n, tiles, owners, total), ou...]
where the time goes in v7:
time: 22 us; the launch traced here: 21.9 us
  Pallas kernels  21.2 us (96%)
  between operations  0.64 us (3%)
    pallas_call x1, Pallas kernels, shards(): pl.pallas_call(functools.partial(body, plan, n, tiles, owners, total), ou...  20.2 us
    pallas_call x1, Pallas kernels, shards(): pl.pallas_call(store, out_shape=(jax.ShapeDtypeStruct((rows, channels), B...  1.05 us

profile of v7, /device:TPU:0, one launch (start us, length us, event | category | flops | bytes accessed | tf_op | source)
XLA Modules:
  0.0 21.9 jit_solution(15120774954888845654)
XLA Ops:
  0.6 20.2 %shard_map.155 = (bf16[256,1024]{1,0:T(8,128)(2,1)S(1)}, bf16[256,1024]{1,0:T(8,128)(2,1)S(1)}, f32[31,1024]{1,0:T(8,128)S(1)}, f32[16,128]{1,0:T(8,128)S(1)}) custom-call(bf16[256,1024]{1,0:T(8,128)(2,1)} %value_h.1, bf16[256,1024]{1,0:T(8,128)(2,1)} %gate_h.1, f32[31,1024]{1,0:T(8,128)} %taps_h.1, f32[1,1024]{1,0:T(1,128)} %bitcast.4, f32[1,1024]{1,0:T(1,128)} %bitcast.5, ...), custom_call_target="tpu_custom_call" | custom-call | tf_op jit(solution)/shard_map/pallas_call | solution.py:696
  20.8 1.1 %shard_map.156 = (bf16[256,1024]{1,0:T(8,128)(2,1)}, bf16[256,1024]{1,0:T(8,128)(2,1)}, f32[31,1024]{1,0:T(8,128)}, f32[8,128]{1,0:T(8,128)}, f32[8,128]{1,0:T(8,128)}) custom-call(bf16[256,1024]{1,0:T(8,128)(2,1)S(1)} %get-tuple-element.14.refs_0_, bf16[256,1024]{1,0:T(8,128)(2,1)S(1)} %get-tuple-element.15.refs_1_, ...), custom_call_target="tpu_custom_call" | custom-call | tf_op jit(solution)/shard_map/pallas_call | solution.py:761
